TPU v7x, 256 devices: a whole 4x4x8 slice. The times are simulated.
256 devices in a mesh: ep: 128 (over z, y, x_hi, core), tp: 2 (over x_lo).
Axes of the slice: x: 4 (x_hi: 2, x_lo: 2; x = x_hi * 2 + x_lo), y: 4, z: 8, core: 2. Of those that a mesh axis runs over, the one named last changes fastest.
Arguments:
- tokens: bfloat16 [1536, 2048], P('ep'), may hold values from -6 to 6
- norm_gain: float32 [2048], replicated, may hold values from 0.1 to 1.9
- w_query: bfloat16 [2048, 768], P(None, 'tp'), may hold values from -0.125 to 0.125
- w_key: bfloat16 [2048, 768], P(None, 'tp'), may hold values from -0.125 to 0.125
- w_value: bfloat16 [2048, 768], P(None, 'tp'), may hold values from -0.125 to 0.125
- w_outgate: bfloat16 [2048, 768], P(None, 'tp'), may hold values from -0.125 to 0.125
- w_input_gate: bfloat16 [2048, 4], replicated, may hold values from -0.125 to 0.125
- w_forget_gate: bfloat16 [2048, 4], replicated, may hold values from -0.125 to 0.125
- forget_bias: float32 [4], replicated, may hold values from -1 to 4
- head_gain: float32 [768], replicated, may hold values from 0.1 to 1.9
- w_output: bfloat16 [768, 2048], P('tp'), may hold values from -0.21875 to 0.21875
- memory: float32 [1536, 4, 192, 192], P('ep', 'tp'), may hold values from -2 to 2
- normalizer: float32 [1536, 4, 192], P('ep', 'tp'), may hold values from -2 to 2
- stabilizer: float32 [1536, 4], P('ep', 'tp'), may hold values from -2 to 2
- ffn_gain: float32 [2048], replicated, may hold values from 0.1 to 1.9
- route_ids: int32 [1536, 4], P('ep'), may hold values from 0 to 127, all different within a row; in each aligned block of 12 rows (0 to 11, 12 to 23, ...) at most 2 rows name the same one
- route_probs: float32 [1536, 4], P('ep'), may hold values from 0.05 to 1
- expert_gate: bfloat16 [128, 2048, 1024], P('ep', None, 'tp'), may hold values from -0.125 to 0.125
- expert_up: bfloat16 [128, 2048, 1024], P('ep', None, 'tp'), may hold values from -0.125 to 0.125
- expert_down: bfloat16 [128, 1024, 2048], P('ep', 'tp'), may hold values from -0.1875 to 0.1875
Outputs:
- next_tokens: bfloat16 [1536, 2048], P('ep')
- new_memory: float32 [1536, 4, 192, 192], P('ep', 'tp')
- new_normalizer: float32 [1536, 4, 192], P('ep', 'tp')
- new_stabilizer: float32 [1536, 4], P('ep', 'tp')
Inputs may be any that keep to these rules, and one draw needn't show every extreme that they name: `route_ids`: in each aligned block of 12 rows (the rows of one index of ep), no expert appears more than 2 times among the block's routes, and some expert appears exactly 2 times; the 4 experts of a row are different.
All inputs are finite; a program needn't handle non-finite values.
Results may differ from a plain program's by a relative error of at most 0.015.
Values may be sent and summed in bfloat16 or wider, within the bound.
A program may use at most 128 MiB of HBM per device.

v0:
```python
import jax
import jax.numpy as jnp
from jax import lax
from jax.sharding import PartitionSpec as P

EPS = 1e-06


def from_everyone(shard, axis):
    copies = jnp.broadcast_to(shard, (lax.axis_size(axis), *shard.shape))
    return lax.all_to_all(copies, axis, split_axis=0, concat_axis=0, tiled=True)


def of_everyone(shard, axis):
    everything = from_everyone(shard, axis)
    return jnp.sum(everything.astype(jnp.float32), axis=0)


def rms_scaled(values, scales):
    floats = values.astype(jnp.float32)
    return floats * lax.rsqrt(jnp.mean(floats * floats, axis=-1, keepdims=True) + EPS) * scales


def local(
    tokens,
    norm_gain,
    w_query,
    w_key,
    w_value,
    w_outgate,
    w_input_gate,
    w_forget_gate,
    forget_bias,
    head_gain,
    w_output,
    memory,
    normalizer,
    stabilizer,
    ffn_gain,
    route_ids,
    route_probs,
    expert_gate,
    expert_up,
    expert_down,
):
    tp_rank = lax.axis_index("tp")
    ep_count = lax.axis_size("ep")
    dev_rows, width = tokens.shape
    dev_heads = memory.shape[1]
    head_dim = memory.shape[2]
    local_width = dev_heads * head_dim
    normed = rms_scaled(tokens, norm_gain).astype(jnp.bfloat16)
    query = jnp.dot(normed, w_query, preferred_element_type=jnp.float32)
    key_raw = jnp.dot(normed, w_key, preferred_element_type=jnp.float32)
    value_raw = jnp.dot(normed, w_value, preferred_element_type=jnp.float32)
    outgate = jnp.dot(normed, w_outgate, preferred_element_type=jnp.float32)
    head_start = tp_rank * dev_heads
    input_cols = lax.dynamic_slice_in_dim(w_input_gate, head_start, dev_heads, 1)
    forget_cols = lax.dynamic_slice_in_dim(w_forget_gate, head_start, dev_heads, 1)
    bias_part = lax.dynamic_slice_in_dim(forget_bias, head_start, dev_heads, 0)
    gain_part = lax.dynamic_slice_in_dim(head_gain, tp_rank * local_width, local_width, 0)
    query = query.reshape(dev_rows, dev_heads, head_dim)
    key_vec = (key_raw * head_dim ** (-0.5)).reshape(dev_rows, dev_heads, head_dim)
    value_vec = value_raw.reshape(dev_rows, dev_heads, head_dim)
    input_pre = jnp.dot(normed, input_cols, preferred_element_type=jnp.float32)
    log_forget = jax.nn.log_sigmoid(
        jnp.dot(normed, forget_cols, preferred_element_type=jnp.float32) + bias_part
    )
    new_stab = jnp.maximum(log_forget + stabilizer, input_pre)
    keep_gate = jnp.exp(log_forget + stabilizer - new_stab)
    write_gate = jnp.exp(input_pre - new_stab)
    new_memory = (
        keep_gate[:, :, None, None] * memory
        + write_gate[:, :, None, None] * key_vec[:, :, :, None] * value_vec[:, :, None, :]
    )
    new_normalizer = keep_gate[:, :, None] * normalizer + write_gate[:, :, None] * key_vec
    numerator = jnp.einsum("bhd,bhde->bhe", query, new_memory)
    denominator = jnp.sum(query * new_normalizer, axis=-1)
    readout = numerator / jnp.maximum(jnp.abs(denominator), jnp.exp(-new_stab))[:, :, None]
    normed_read = (
        readout
        * lax.rsqrt(jnp.mean(readout * readout, axis=-1, keepdims=True) + EPS)
        * gain_part.reshape(dev_heads, head_dim)
    )
    gated = (normed_read.reshape(dev_rows, local_width) * jax.nn.sigmoid(outgate)).astype(
        jnp.bfloat16
    )
    partial_value = jnp.dot(gated, w_output, preferred_element_type=jnp.float32).astype(
        jnp.bfloat16
    )
    mixed = (
        of_everyone(partial_value.astype(jnp.float32).astype(jnp.bfloat16), "tp")
        .astype(jnp.float32)
        .astype(jnp.bfloat16)
    )
    resid = (tokens.astype(jnp.float32) + mixed.astype(jnp.float32)).astype(jnp.bfloat16)
    ffn_in = rms_scaled(resid, ffn_gain).astype(jnp.bfloat16)
    weights = route_probs / jnp.sum(route_probs, axis=-1, keepdims=True)
    top_count = route_ids.shape[1]
    experts_total = ep_count * expert_gate.shape[0]
    capacity = max(2, 2 * dev_rows * top_count // experts_total)
    flat_expert = route_ids.reshape(-1)
    onehot = (flat_expert[:, None] == jnp.arange(experts_total, dtype=jnp.int32)[None, :]).astype(
        jnp.int32
    )
    earlier = jnp.cumsum(onehot, axis=0) - onehot
    slot_rank = jnp.sum(earlier * onehot, axis=-1)
    position = flat_expert * capacity + slot_rank
    select = (
        jnp.arange(experts_total * capacity, dtype=jnp.int32)[:, None] == position[None, :]
    ).astype(jnp.bfloat16)
    repeated = jnp.repeat(ffn_in, top_count, axis=0)
    outgoing = jnp.dot(select, repeated, preferred_element_type=jnp.float32).astype(jnp.bfloat16)
    outgoing = outgoing.reshape(experts_total, 1, capacity, width)
    incoming = lax.all_to_all(outgoing, "ep", split_axis=0, concat_axis=1, tiled=True)
    gate_val = jnp.einsum(
        "esnd,edf->esnf", incoming, expert_gate, preferred_element_type=jnp.float32
    )
    up_val = jnp.einsum("esnd,edf->esnf", incoming, expert_up, preferred_element_type=jnp.float32)
    hidden = (jax.nn.silu(gate_val) * up_val).astype(jnp.bfloat16)
    partial_out = jnp.einsum(
        "esnf,efd->esnd", hidden, expert_down, preferred_element_type=jnp.float32
    ).astype(jnp.bfloat16)
    served = (
        of_everyone(partial_out.astype(jnp.float32).astype(jnp.bfloat16), "tp")
        .astype(jnp.float32)
        .astype(jnp.bfloat16)
    )
    returned = lax.all_to_all(served, "ep", split_axis=1, concat_axis=0, tiled=True).reshape(
        experts_total * capacity, width
    )
    picked = jnp.dot(select.T, returned, preferred_element_type=jnp.float32).reshape(
        dev_rows, top_count, width
    )
    combined = jnp.sum(picked * weights[:, :, None], axis=1)
    next_tokens = (resid.astype(jnp.float32) + combined).astype(jnp.bfloat16)
    return (next_tokens, new_memory, new_normalizer, new_stab)


def solution(mesh):
    return jax.shard_map(
        local,
        mesh=mesh,
        in_specs=(
            P("ep", None),
            P(),
            P(None, "tp"),
            P(None, "tp"),
            P(None, "tp"),
            P(None, "tp"),
            P(),
            P(),
            P(),
            P(),
            P("tp", None),
            P("ep", "tp", None, None),
            P("ep", "tp", None),
            P("ep", "tp"),
            P(),
            P("ep", None),
            P("ep", None),
            P("ep", None, "tp"),
            P("ep", None, "tp"),
            P("ep", "tp", None),
        ),
        out_specs=(P("ep", None), P("ep", "tp", None, None), P("ep", "tp", None), P("ep", "tp")),
        check_vma=False,
    )
```

profile of v0, /device:TPU:4, one launch (start us, length us, event | category | flops | bytes accessed | tf_op | source)
XLA Modules:
  0.0 155.6 jit_solution(14123573286189916450)
XLA Ops:
  0.7 1.1 fusion.33
  1.8 1.8 %fusion.63 = f32[12,384]{1,0:T(8,128)S(1)} fusion(bf16[2048,384]{1,0:T(8,128)(2,1)} %param.22, bf16[12,2048]{1,0:T(8,128)(2,1)} %param.20, f32[2048]{0:T(1024)} %param.21, f32[12]{0:T(128)S(1)} %add_rsqrt_fusion.2), kind=kOutput, calls=%fused_computation.79 | convolution fusion | flops 18972672 | bytes 1648688 | tf_op jit(solution)/shard_map/dot_general | solution.py:53
  3.8 1.1 fusion.45
  4.9 0.7 dynamic_slice.13
  5.6 1.1 subtract_exponential_fusion.1
  6.9 1.8 %convolution_multiply_fusion.1 = f32[12,384]{1,0:T(8,128)S(1)} fusion(bf16[2048,384]{1,0:T(8,128)(2,1)} %param.23, bf16[12,2048]{1,0:T(8,128)(2,1)S(1)} %copy-done.2, f32[2048]{0:T(1024)S(1)} %copy-done.4, f32[12]{0:T(128)S(1)} %add_rsqrt_fusion.2), kind=kOutput, calls=%fused_computation.17 | convolution fusion | flops 18977280 | bytes 1648688 | tf_op jit(solution)/shard_map/dot_general | solution.py:54
  8.8 1.8 %fusion.58 = f32[12,384]{1,0:T(8,128)S(1)} fusion(bf16[2048,384]{1,0:T(8,128)(2,1)} %param.24, bf16[12,2048]{1,0:T(8,128)(2,1)S(1)} %copy-done.2, f32[2048]{0:T(1024)S(1)} %copy-done.4, f32[12]{0:T(128)S(1)} %add_rsqrt_fusion.2), kind=kOutput, calls=%fused_computation.78 | convolution fusion | flops 18972672 | bytes 1648688 | tf_op jit(solution)/shard_map/dot_general | solution.py:55
  10.7 0.7 multiply_reduce_fusion.1
  11.6 2.8 %multiply_add_fusion = f32[12,2,192,192]{3,2,1,0:T(8,128)S(1)} fusion(f32[12,2,192,192]{3,2,1,0:T(8,128)} %param.31, f32[12,2,192]{2,1,0:T(2,128)S(1)} %mul.168, f32[12,2,192]{2,1,0:T(2,128)S(1)} %get-tuple-element.8, f32[12,2]{1,0:T(8,128)S(1)} %copy.59), kind=kLoop, calls=%fused_computation | loop fusion | flops 2654208 | bytes 7114848 | tf_op jit(solution)/shard_map/add | solution.py:73
  14.4 0.4 fusion.65
  14.8 1.7 %copy-done.1 = f32[12,2,192,192]{3,2,1,0:T(8,128)} copy-done((f32[12,2,192,192]{3,2,1,0:T(8,128)}, f32[12,2,192,192]{3,2,1,0:T(8,128)S(1)}, u32[]{:S(2)}) %copy-start.1) | copy-done | bytes 3538968
  16.6 0.2 multiply_reduce_fusion
  17.1 2.7 %convolution_convert_fusion.2 = bf16[12,2048]{1,0:T(8,128)(2,1)S(1)} fusion(bf16[384,2048]{1,0:T(8,128)(2,1)} %param.30, f32[12,384]{1,0:T(8,128)S(1)} %reshape.146, bf16[2048,384]{1,0:T(8,128)(2,1)} %param.25, bf16[12,2048]{1,0:T(8,128)(2,1)S(1)} %copy-done.2, f32[2048]{0:T(1024)S(1)} %copy-done.4, f32[12]{0:T(128)S(1)} %add_rsqrt_fusion.2), kind=kOutput, calls=%fused_computation.4 | convolution fusion | flops 37894656 | bytes 3270704 | tf_op jit(solution)/shard_map/dot_general | solution.py:88
  19.8 0.7 broadcast_in_dim.6
  20.4 3.4 %all-to-all-start = ((bf16[2,12,2048]{2,1,0:T(8,128)(2,1)}), bf16[2,12,2048]{2,1,0:T(8,128)(2,1)S(1)}, u32[]{:S(2)}, u32[]{:S(2)}) async-start(bf16[2,12,2048]{2,1,0:T(8,128)(2,1)} %broadcast_in_dim.6), calls=%async_computation | async-start | bytes 262144 | tf_op jit(solution)/shard_map/all_to_all | solution.py:11
  24.2 0.2 select_reduce_fusion
  24.4 3.9 %all-to-all-done = bf16[2,12,2048]{2,1,0:T(8,128)(2,1)S(1)} async-done(((bf16[2,12,2048]{2,1,0:T(8,128)(2,1)}), bf16[2,12,2048]{2,1,0:T(8,128)(2,1)S(1)}, u32[]{:S(2)}, u32[]{:S(2)}) %all-to-all-start) | async-done | bytes 98336 | tf_op jit(solution)/shard_map/all_to_all | solution.py:11
  28.7 0.4 convolution_convert_fusion.1
  29.1 1.5 reshape.149
  30.6 45.1 %all_to_all.28 = bf16[128,1,2,2048]{3,2,1,0:T(2,128)(2,1)S(1)} all-to-all(bf16[128,1,2,2048]{3,2,1,0:T(2,128)(2,1)} %bitcast.42), channel_id=1, replica_groups=mesh['ep'=128,'tp'=2] {'ep'}, dimensions={0} | all-to-all | bytes 2097152 | tf_op jit(solution)/shard_map/all_to_all | solution.py:115
  75.7 1.0 copy-done.3
  76.7 1.5 fusion.3
  78.3 3.4 %convolution_convert_fusion = bf16[128,2,2048]{2,0,1:T(8,128)(2,1)S(1)} fusion(bf16[1,512,2048]{2,1,0:T(8,128)(2,1)S(1)} %copy-done, bf16[1,2048,512]{2,1,0:T(8,128)(2,1)} %param.38, bf16[128,1,2,2048]{3,2,1,0:T(2,128)(2,1)} %copy-done.3, f32[128,2,512]{2,0,1:T(8,128)} %fusion.3), kind=kOutput, calls=%fused_computation.1 | convolution fusion | flops 1075052544 | bytes 6815744 | tf_op jit(solution)/shard_map/esnf,efd->esnd/dot_general | solution.py:121
  81.6 0.2 broadcast_in_dim.8
  81.9 27.3 %all_to_all.29 = bf16[2,1,128,2,2048]{4,2,3,1,0:T(8,128)(2,1)} all-to-all(bf16[2,1,128,2,2048]{4,2,3,1,0:T(8,128)(2,1)S(1)} %broadcast_in_dim.8), channel_id=1, replica_groups=mesh['ep'=128,'tp'=2] {'tp'}, dimensions={0} | all-to-all | bytes 4194304 | tf_op jit(solution)/shard_map/all_to_all | solution.py:11
  109.1 2.1 %reduce_sum.95 = bf16[128,2,2048]{2,0,1:T(8,128)(2,1)S(1)} reduce(bf16[2,1,128,2,2048]{4,2,3,1,0:T(8,128)(2,1)} %all_to_all.29, bf16[]{:T(256)} %constant.42.clone.1), dimensions={0,1}, to_apply=%region_7.8 | reduce | flops 524288 | bytes 3145730 | tf_op jit(solution)/shard_map/reduce_sum | solution.py:16
  111.3 2.1 %copy.68 = bf16[1,128,2,2048]{3,2,0,1:T(2,128)(2,1)} copy(bf16[1,128,2,2048]{3,1,2,0:T(8,128)(2,1)S(1)} %bitcast.41) | data formatting | bytes 2097152 | tf_op jit(solution)/shard_map/reduce_sum | solution.py:16
  113.3 9.3 %all-to-all-start.3 = ((bf16[1,128,2,2048]{3,2,0,1:T(2,128)(2,1)}), bf16[1,128,2,2048]{3,2,0,1:T(2,128)(2,1)S(1)}, u32[]{:S(2)}, u32[]{:S(2)}) async-start(bf16[1,128,2,2048]{3,2,0,1:T(2,128)(2,1)} %copy.68), calls=%async_computation.3 | async-start | bytes 2097152 | tf_op jit(solution)/shard_map/all_to_all | solution.py:129
  122.8 29.4 %all-to-all-done.3 = bf16[1,128,2,2048]{3,2,0,1:T(2,128)(2,1)S(1)} async-done(((bf16[1,128,2,2048]{3,2,0,1:T(2,128)(2,1)}), bf16[1,128,2,2048]{3,2,0,1:T(2,128)(2,1)S(1)}, u32[]{:S(2)}, u32[]{:S(2)}) %all-to-all-start.3) | async-done | bytes 1048608 | tf_op jit(solution)/shard_map/all_to_all | solution.py:129
  152.2 1.2 reshape.160
  153.4 1.5 fusion.11
  155.0 0.7 fusion.40
  (53 shorter events, 2.0 us)
Async XLA Ops:
  0.6 77.6 %copy-start = (bf16[1,512,2048]{2,1,0:T(8,128)(2,1)S(1)}, bf16[1,512,2048]{2,1,0:T(8,128)(2,1)}, u32[]{:S(2)}) copy-start(bf16[1,512,2048]{2,1,0:T(8,128)(2,1)} %param.39) | copy-start | bytes 6291460
  0.6 6.3 %copy-start.2 = (bf16[12,2048]{1,0:T(8,128)(2,1)S(1)}, bf16[12,2048]{1,0:T(8,128)(2,1)}, u32[]{:S(2)}) copy-start(bf16[12,2048]{1,0:T(8,128)(2,1)} %param.20) | copy-start | bytes 147460
  0.7 6.3 %copy-start.4 = (f32[2048]{0:T(1024)S(1)}, f32[2048]{0:T(1024)}, u32[]{:S(2)}) copy-start(f32[2048]{0:T(1024)} %param.21) | copy-start | bytes 24580
  3.6 7.0 %copy-start.5 = (f32[12,2,192]{2,1,0:T(2,128)S(1)}, f32[12,2,192]{2,1,0:T(2,128)}, u32[]{:S(2)}) copy-start(f32[12,2,192]{2,1,0:T(2,128)} %param.32) | copy-start | bytes 55300
  6.7 7.7 %copy-start.8 = (f32[12,2]{0,1:T(2,128)}, f32[12,2]{0,1:T(2,128)S(1)}, u32[]{:S(2)}) copy-start(f32[12,2]{0,1:T(2,128)S(1)} %get-tuple-element.10) | copy-start | bytes 292
  14.4 2.2 %copy-start.1 = (f32[12,2,192,192]{3,2,1,0:T(8,128)}, f32[12,2,192,192]{3,2,1,0:T(8,128)S(1)}, u32[]{:S(2)}) copy-start(f32[12,2,192,192]{3,2,1,0:T(8,128)S(1)} %multiply_add_fusion) | copy-start | bytes 10616836
  14.4 2.4 %copy-start.10 = (f32[768]{0:T(1024)S(1)}, f32[768]{0:T(1024)}, u32[]{:S(2)}) copy-start(f32[768]{0:T(1024)} %param.29) | copy-start | bytes 9220
  16.6 7.3 %copy-start.9 = (s32[12,4]{0,1:T(4,128)S(1)}, s32[12,4]{0,1:T(4,128)}, u32[]{:S(2)}) copy-start(s32[12,4]{0,1:T(4,128)} %param.35) | copy-start | bytes 580
  17.1 11.4 %copy-start.6 = (f32[2048]{0:T(1024)S(1)}, f32[2048]{0:T(1024)}, u32[]{:S(2)}) copy-start(f32[2048]{0:T(1024)} %param.34) | copy-start | bytes 24580
  20.4 7.8 %all-to-all-start = ((bf16[2,12,2048]{2,1,0:T(8,128)(2,1)}), bf16[2,12,2048]{2,1,0:T(8,128)(2,1)S(1)}, u32[]{:S(2)}, u32[]{:S(2)}) async-start(bf16[2,12,2048]{2,1,0:T(8,128)(2,1)} %broadcast_in_dim.6), calls=%async_computation | async-start | bytes 262144 | tf_op jit(solution)/shard_map/all_to_all | solution.py:11
  30.6 46.1 %copy-start.11 = (bf16[1,2048,512]{2,1,0:T(8,128)(2,1)S(1)}, bf16[1,2048,512]{2,1,0:T(8,128)(2,1)}, u32[]{:S(2)}) copy-start(bf16[1,2048,512]{2,1,0:T(8,128)(2,1)} %param.37) | copy-start | bytes 6291460
  75.7 1.0 copy-start.3
  111.3 11.5 %copy-start.7 = (f32[12,4]{0,1:T(4,128)S(1)}, f32[12,4]{0,1:T(4,128)}, u32[]{:S(2)}) copy-start(f32[12,4]{0,1:T(4,128)} %param.36) | copy-start | bytes 580
  113.3 38.9 %all-to-all-start.3 = ((bf16[1,128,2,2048]{3,2,0,1:T(2,128)(2,1)}), bf16[1,128,2,2048]{3,2,0,1:T(2,128)(2,1)S(1)}, u32[]{:S(2)}, u32[]{:S(2)}) async-start(bf16[1,128,2,2048]{3,2,0,1:T(2,128)(2,1)} %copy.68), calls=%async_computation.3 | async-start | bytes 2097152 | tf_op jit(solution)/shard_map/all_to_all | solution.py:129
where the time goes:
time: 159 us; the launch traced here: 156 us
  blocking collectives  72.3 us (45%)
  waiting for transfers between devices  33.3 us (21%)
  matrix products  17.4 us (11%)
  starting transfers between devices  12.7 us (8%)
  local copies, waits for them, and re-layouts  10.5 us (7%)
  other arithmetic  8.37 us (5%)
    all_to_all x1, blocking collectives, local(): lax.all_to_all(outgoing, 'ep', split_axis=0, concat_axis=1, tiled=True)  45.1 us
    all_to_all x1, waiting for transfers between devices, local(): lax.all_to_all(served, 'ep', split_axis=1, concat_axis=0, tiled=True)  29.4 us
    all_to_all x1, blocking collectives, from_everyone(): return lax.all_to_all(copies, axis, split_axis=0, concat_axis=0, tiled=True)  27.3 us
    all_to_all x1, starting transfers between devices, local(): lax.all_to_all(served, 'ep', split_axis=1, concat_axis=0, tiled=True)  9.32 us
    all_to_all x1, waiting for transfers between devices, from_everyone(): return lax.all_to_all(copies, axis, split_axis=0, concat_axis=0, tiled=True)  3.92 us
    all_to_all x1, starting transfers between devices, from_everyone(): return lax.all_to_all(copies, axis, split_axis=0, concat_axis=0, tiled=True)  3.38 us
    dot_general x1, matrix products, local(): jnp.einsum('esnf,efd->esnd', hidden, expert_down, preferred_element_type=...  3.37 us
  transfers between devices with their start and end apart: 2, of which 2 were waited for; matrix products, arithmetic and copies ran while one was open for 0% of the time, Pallas kernels for 0%

commit v1 on v0

v1 whole, which is shorter than its diff:
```python
import functools

import jax
import jax.numpy as jnp
from jax import lax
from jax.experimental import pallas as pl
from jax.experimental.pallas import tpu as pltpu
from jax.sharding import PartitionSpec as P

EPS = 1e-06
PLANE = 16
BF16 = jnp.bfloat16
F32 = jnp.float32


def rms_scaled(values, scales):
    floats = values.astype(F32)
    return floats * lax.rsqrt(jnp.mean(floats * floats, axis=-1, keepdims=True) + EPS) * scales


def moe_kernel(
    nz,
    ng,
    part_ref,
    tok_ref,
    gain_ref,
    meta_ref,
    wg_hbm,
    wu_hbm,
    wd_hbm,
    out_ref,
    wg,
    wu,
    wd,
    pbuf,
    meta,
    zrows,
    snd,
    rcv,
    osnd,
    back,
    zsnd,
    zrcv,
    hbuf,
    w_sem,
    p_sem,
    m_sem,
    z_sem,
    d_sem,
    b_sem,
    r_sem,
    f_sem,
):
    ep = lax.axis_index("ep")
    tp = lax.axis_index("tp")
    z = ep // ng
    g = ep % ng
    me = g * 2 + tp
    other = 1 - tp
    np_ = 2 * ng
    rows = tok_ref.shape[0]
    half = tok_ref.shape[1] // 2
    slots = 2 * nz

    weights = [
        pltpu.make_async_copy(src, dst, w_sem.at[i])
        for i, (src, dst) in enumerate(((wg_hbm, wg), (wu_hbm, wu), (wd_hbm, wd)))
    ]
    for copy in weights:
        copy.start()

    barrier = pltpu.get_barrier_semaphore()

    @pl.loop(1, nz)
    def _(d):
        pl.semaphore_signal(barrier, inc=1, device_id=(lax.rem(z + d, nz) * ng + g, tp))

    @pl.loop(1, np_)
    def _(d):
        q = lax.rem(me + d, np_)
        pl.semaphore_signal(barrier, inc=1, device_id=(z * ng + q // 2, q % 2))

    pl.semaphore_wait(barrier, nz - 1 + np_ - 1)

    def remote(src, dst, sems, at_src, at_dst, to_ep, to_tp):
        return pltpu.make_async_remote_copy(
            src_ref=src,
            dst_ref=dst,
            send_sem=sems.at[0, at_src],
            recv_sem=sems.at[1, at_dst],
            device_id=(to_ep, to_tp),
        )

    swap = remote(part_ref, pbuf, p_sem, 0, 0, ep, other)
    swap.start()

    def meta_copy(d, at):
        to = lax.rem(z + d, nz)
        return remote(meta_ref, meta.at[at], m_sem, d, at, to * ng + g, tp)

    @pl.loop(1, nz)
    def _(d):
        meta_copy(d, z).start()

    meta[z] = meta_ref[...]

    @pl.loop(1, nz)
    def _(d):
        meta_copy(d, lax.rem(z + d, nz)).wait_recv()

    base = (z * (ng * slots) + 1).astype(F32)
    code_t = meta[0][rows:, :]
    for s in range(1, nz):
        code_t = code_t + meta[s][rows:, :]
    code_t = (code_t - base).astype(jnp.int32)
    lanes = nz * rows
    slot_at = lax.broadcasted_iota(jnp.int32, (ng * slots, lanes), 0)
    pick = jnp.zeros((ng * slots, lanes), F32)
    for k in range(4):
        pick = pick + jnp.where(slot_at == code_t[k : k + 1, :lanes], 1.0, 0.0)
    pick = pick.astype(BF16)
    by_row = meta[:, :rows, :].reshape(lanes, meta.shape[2])
    code_r = (by_row[:, 0:4] - base).astype(jnp.int32)
    slot_at = lax.broadcasted_iota(jnp.int32, (lanes, ng * slots), 1)
    mix = jnp.zeros((lanes, ng * slots), F32)
    for k in range(4):
        mix = mix + jnp.where(slot_at == code_r[:, k : k + 1], by_row[:, 4 + k : 5 + k], 0.0)
    mix_hi = mix.astype(BF16)
    mix_lo = (mix - mix_hi.astype(F32)).astype(BF16)

    swap.wait_recv()
    mixed = (part_ref[...].astype(F32) + pbuf[...].astype(F32)).astype(BF16)
    resid = (tok_ref[...].astype(F32) + mixed.astype(F32)).astype(BF16)
    ffn_in = rms_scaled(resid, gain_ref[...]).astype(BF16)

    def my_half(values):
        return jnp.where(tp == 0, values[:, :half], values[:, half:])

    zrows[z] = my_half(ffn_in)

    def z_copy(d, at):
        to = lax.rem(z + d, nz)
        return remote(zrows.at[z], zrows.at[at], z_sem, d, at, to * ng + g, tp)

    @pl.loop(1, nz)
    def _(d):
        z_copy(d, z).start()

    @pl.loop(1, nz)
    def _(d):
        z_copy(d, lax.rem(z + d, nz)).wait_recv()

    gathered = zrows[...].reshape(lanes, half)
    snd[...] = (
        jnp.dot(pick, gathered, preferred_element_type=F32).astype(BF16).reshape(ng, slots, half)
    )

    def d_copy(d, at):
        q = lax.rem(me + d, np_)
        to_g, to_tp = q // 2, q % 2
        return remote(
            snd.at[to_g], rcv.at[at % 2, at // 2], d_sem, d, at, z * ng + to_g, to_tp
        )

    @pl.loop(1, np_)
    def _(d):
        d_copy(d, me).start()

    rcv[tp, g] = snd[g]
    for copy in weights:
        copy.wait()

    @pl.loop(1, np_)
    def _(d):
        d_copy(d, lax.rem(me + d, np_)).wait_recv()

    left = rcv[0].reshape(ng * slots, half)
    right = rcv[1].reshape(ng * slots, half)

    def both(w):
        return jnp.dot(left, w[:half, :], preferred_element_type=F32) + jnp.dot(
            right, w[half:, :], preferred_element_type=F32
        )

    gate_val = both(wg)
    hidden = (gate_val * jax.nn.sigmoid(gate_val) * both(wu)).astype(BF16)
    for h in range(2):
        osnd[h] = (
            jnp.dot(hidden, wd[:, h * half : (h + 1) * half], preferred_element_type=F32)
            .astype(BF16)
            .reshape(ng, slots, half)
        )

    def b_copy(d, at):
        q = lax.rem(me + d, np_)
        to_g, to_tp = q // 2, q % 2
        return remote(
            osnd.at[to_tp, to_g], back.at[at % 2, at // 2], b_sem, d, at, z * ng + to_g, to_tp
        )

    @pl.loop(1, np_)
    def _(d):
        b_copy(d, me).start()

    back[tp, g] = osnd[tp, g]

    @pl.loop(1, np_)
    def _(d):
        b_copy(d, lax.rem(me + d, np_)).wait_recv()

    served = (back[0].astype(F32) + back[1].astype(F32)).astype(BF16).reshape(ng * slots, half)
    sums = jnp.dot(mix_hi, served, preferred_element_type=F32) + jnp.dot(
        mix_lo, served, preferred_element_type=F32
    )
    zsnd[...] = sums.astype(BF16).reshape(nz, rows, half)

    def r_copy(d, at):
        to = lax.rem(z + d, nz)
        return remote(zsnd.at[to], zrcv.at[at], r_sem, d, at, to * ng + g, tp)

    @pl.loop(1, nz)
    def _(d):
        r_copy(d, z).start()

    zrcv[z] = zsnd[z]

    @pl.loop(1, nz)
    def _(d):
        r_copy(d, lax.rem(z + d, nz)).wait_recv()

    total = my_half(resid).astype(F32)
    for s in range(nz):
        total = total + zrcv[s].astype(F32)
    mine = total.astype(BF16)
    hbuf[0] = mine
    last = remote(hbuf.at[0], hbuf.at[1], f_sem, 0, 0, ep, other)
    last.start()
    last.wait_recv()
    theirs = hbuf[1]
    real = out_ref.shape[0]
    out_ref[:, :half] = jnp.where(tp == 0, mine, theirs)[:real]
    out_ref[:, half:] = jnp.where(tp == 0, theirs, mine)[:real]

    swap.wait_send()
    last.wait_send()

    @pl.loop(1, nz)
    def _(d):
        meta_copy(d, z).wait_send()
        z_copy(d, z).wait_send()
        r_copy(d, z).wait_send()

    @pl.loop(1, np_)
    def _(d):
        d_copy(d, me).wait_send()
        b_copy(d, me).wait_send()


def moe(nz, ng, part, tok, gain, meta, wg, wu, wd, real):
    rows, width = tok.shape
    half = width // 2
    slots = 2 * nz
    vmem = pl.BlockSpec(memory_space=pltpu.VMEM)
    hbm = pl.BlockSpec(memory_space=pl.ANY)

    def sems(n):
        return pltpu.SemaphoreType.DMA((2, n))

    return pl.pallas_call(
        functools.partial(moe_kernel, nz, ng),
        out_shape=jax.ShapeDtypeStruct((real, width), BF16),
        in_specs=[vmem] * 4 + [hbm] * 3,
        out_specs=vmem,
        scratch_shapes=[
            pltpu.VMEM(wg.shape, BF16),
            pltpu.VMEM(wu.shape, BF16),
            pltpu.VMEM(wd.shape, BF16),
            pltpu.VMEM((rows, width), BF16),
            pltpu.VMEM((nz, *meta.shape), F32),
            pltpu.VMEM((nz, rows, half), BF16),
            pltpu.VMEM((ng, slots, half), BF16),
            pltpu.VMEM((2, ng, slots, half), BF16),
            pltpu.VMEM((2, ng, slots, half), BF16),
            pltpu.VMEM((2, ng, slots, half), BF16),
            pltpu.VMEM((nz, rows, half), BF16),
            pltpu.VMEM((nz, rows, half), BF16),
            pltpu.VMEM((2, rows, half), BF16),
            pltpu.SemaphoreType.DMA((3,)),
            sems(1),
            sems(nz),
            sems(nz),
            sems(2 * ng),
            sems(2 * ng),
            sems(nz),
            sems(1),
        ],
        compiler_params=pltpu.CompilerParams(
            collective_id=0, has_side_effects=True, vmem_limit_bytes=48 << 20
        ),
        name="experts",
    )(part, tok, gain, meta, wg, wu, wd)


def route_meta(z, nz, rows, route_ids, route_probs):
    count, top = route_ids.shape
    same = route_ids[:, :, None, None] == route_ids[None, None, :, :]
    before = jnp.arange(count)[None, :] < jnp.arange(count)[:, None]
    rank = jnp.sum((same & before[:, None, :, None]).astype(jnp.int32), axis=(2, 3))
    code = (route_ids * (2 * nz) + 2 * z + rank + 1).astype(F32)
    weights = route_probs / jnp.sum(route_probs, axis=-1, keepdims=True)
    by_row = jnp.pad(jnp.concatenate([code, weights], axis=1), ((0, rows - count), (0, 128 - 2 * top)))
    spread = (jnp.arange(nz) == z).astype(F32)[None, :, None] * jnp.pad(
        code.T, ((0, 8 - top), (0, rows - count))
    )[:, None, :]
    by_lane = jnp.pad(spread.reshape(8, nz * rows), ((0, 0), (0, 128 - nz * rows)))
    return jnp.concatenate([by_row, by_lane], axis=0)


def local(
    tokens,
    norm_gain,
    w_query,
    w_key,
    w_value,
    w_outgate,
    w_input_gate,
    w_forget_gate,
    forget_bias,
    head_gain,
    w_output,
    memory,
    normalizer,
    stabilizer,
    ffn_gain,
    route_ids,
    route_probs,
    expert_gate,
    expert_up,
    expert_down,
):
    tp_rank = lax.axis_index("tp")
    ep_count = lax.axis_size("ep")
    ng = min(PLANE, ep_count // 2)
    nz = ep_count // ng
    dev_rows, width = tokens.shape
    dev_heads = memory.shape[1]
    head_dim = memory.shape[2]
    local_width = dev_heads * head_dim
    normed = rms_scaled(tokens, norm_gain).astype(jnp.bfloat16)
    query = jnp.dot(normed, w_query, preferred_element_type=jnp.float32)
    key_raw = jnp.dot(normed, w_key, preferred_element_type=jnp.float32)
    value_raw = jnp.dot(normed, w_value, preferred_element_type=jnp.float32)
    outgate = jnp.dot(normed, w_outgate, preferred_element_type=jnp.float32)
    head_start = tp_rank * dev_heads
    input_cols = lax.dynamic_slice_in_dim(w_input_gate, head_start, dev_heads, 1)
    forget_cols = lax.dynamic_slice_in_dim(w_forget_gate, head_start, dev_heads, 1)
    bias_part = lax.dynamic_slice_in_dim(forget_bias, head_start, dev_heads, 0)
    gain_part = lax.dynamic_slice_in_dim(head_gain, tp_rank * local_width, local_width, 0)
    query = query.reshape(dev_rows, dev_heads, head_dim)
    key_vec = (key_raw * head_dim ** (-0.5)).reshape(dev_rows, dev_heads, head_dim)
    value_vec = value_raw.reshape(dev_rows, dev_heads, head_dim)
    input_pre = jnp.dot(normed, input_cols, preferred_element_type=jnp.float32)
    log_forget = jax.nn.log_sigmoid(
        jnp.dot(normed, forget_cols, preferred_element_type=jnp.float32) + bias_part
    )
    new_stab = jnp.maximum(log_forget + stabilizer, input_pre)
    keep_gate = jnp.exp(log_forget + stabilizer - new_stab)
    write_gate = jnp.exp(input_pre - new_stab)
    new_memory = (
        keep_gate[:, :, None, None] * memory
        + write_gate[:, :, None, None] * key_vec[:, :, :, None] * value_vec[:, :, None, :]
    )
    new_normalizer = keep_gate[:, :, None] * normalizer + write_gate[:, :, None] * key_vec
    numerator = jnp.einsum("bhd,bhde->bhe", query, new_memory)
    denominator = jnp.sum(query * new_normalizer, axis=-1)
    readout = numerator / jnp.maximum(jnp.abs(denominator), jnp.exp(-new_stab))[:, :, None]
    normed_read = (
        readout
        * lax.rsqrt(jnp.mean(readout * readout, axis=-1, keepdims=True) + EPS)
        * gain_part.reshape(dev_heads, head_dim)
    )
    gated = (normed_read.reshape(dev_rows, local_width) * jax.nn.sigmoid(outgate)).astype(
        jnp.bfloat16
    )
    rows = -(-dev_rows // 16) * 16
    pad = ((0, rows - dev_rows), (0, 0))
    partial_value = jnp.dot(
        jnp.pad(gated, pad), w_output, preferred_element_type=jnp.float32
    ).astype(jnp.bfloat16)
    meta = route_meta(lax.axis_index("ep") // ng, nz, rows, route_ids, route_probs)
    next_tokens = moe(
        nz,
        ng,
        partial_value,
        jnp.pad(tokens, pad),
        ffn_gain.reshape(1, width),
        meta,
        expert_gate[0],
        expert_up[0],
        expert_down[0],
        dev_rows,
    )
    return (next_tokens, new_memory, new_normalizer, new_stab)


def solution(mesh):
    return jax.shard_map(
        local,
        mesh=mesh,
        in_specs=(
            P("ep", None),
            P(),
            P(None, "tp"),
            P(None, "tp"),
            P(None, "tp"),
            P(None, "tp"),
            P(),
            P(),
            P(),
            P(),
            P("tp", None),
            P("ep", "tp", None, None),
            P("ep", "tp", None),
            P("ep", "tp"),
            P(),
            P("ep", None),
            P("ep", None),
            P("ep", None, "tp"),
            P("ep", None, "tp"),
            P("ep", "tp", None),
        ),
        out_specs=(P("ep", None), P("ep", "tp", None, None), P("ep", "tp", None), P("ep", "tp")),
        check_vma=False,
    )
```

time: 159 us -> 94.7 us (0.60); the launches traced: 156 us -> 94.2 us
  blocking collectives: 72.3 us -> 0 us
  Pallas kernels: 0 us -> 68.7 us
  waiting for transfers between devices: 33.3 us -> 0 us
  starting transfers between devices: 12.7 us -> 0 us
  matrix products: 17.4 us -> 8.75 us
  local copies, waits for them, and re-layouts: 10.5 us -> 8.47 us
    all_to_all x2 -> x0, blocking collectives: 72.3 us -> none  [the longest x1 45.1 us: local(): lax.all_to_all(outgoing, 'ep', split_axis=0, concat_axis=1, tiled=True)]
    pallas_call x0 -> x1, Pallas kernels: none -> 68.7 us  [moe(): pl.pallas_call(functools.partial(moe_kernel, nz, ng), out_shape=jax.Shape...]
    all_to_all x2 -> x0, waiting for transfers between devices: 33.3 us -> none  [the longest x1 29.4 us: local(): lax.all_to_all(served, 'ep', split_axis=1, concat_axis=0, tiled=True)]
    all_to_all x2 -> x0, starting transfers between devices: 12.7 us -> none  [the longest x1 9.32 us: local(): lax.all_to_all(served, 'ep', split_axis=1, concat_axis=0, tiled=True)]
    dot_general x5 -> x2, matrix products: 9.53 us -> 2.24 us  [the longest x1 1.93 us: local(): outgate = jnp.dot(normed, w_outgate, preferred_element_type=jnp.float32)]
    reshape x4 -> x0, local copies, waits for them, and re-layouts: 2.87 us -> none  [the longest x1 1.52 us: local(): outgoing = outgoing.reshape(experts_total, 1, capacity, width)]
    unnamed x25 -> x24, local copies, waits for them, and re-layouts: 2.89 us -> 5.65 us
    reduce_sum x1 -> x0, local copies, waits for them, and re-layouts: 2.07 us -> none  [of_everyone(): return jnp.sum(everything.astype(jnp.float32), axis=0)]
  transfers between devices with their start and end apart: 2 -> 0, of which waited for: 2 -> 0; matrix products, arithmetic and copies ran while one was open for 0% -> 0% of each run, Pallas kernels for 0% -> 0%
where the time goes in v1:
time: 94.7 us; the launch traced here: 94.2 us
  Pallas kernels  68.7 us (73%)
  matrix products  8.75 us (9%)
  local copies, waits for them, and re-layouts  8.47 us (9%)
  other arithmetic  7.36 us (8%)
    pallas_call x1, Pallas kernels, moe(): pl.pallas_call(functools.partial(moe_kernel, nz, ng), out_shape=jax.Shape...  68.7 us
    unnamed x24, local copies, waits for them, and re-layouts  5.65 us
    add x1, other arithmetic, local(): keep_gate[:, :, None, None] * memory  2.8 us
    dot_general x1, matrix products, local(): outgate = jnp.dot(normed, w_outgate, preferred_element_type=jnp.float32)  1.93 us

profile of v1, /device:TPU:4, one launch (start us, length us, event | category | flops | bytes accessed | tf_op | source)
XLA Modules:
  0.0 94.2 jit_solution(16868521145780820003)
XLA Ops:
  0.7 0.9 dynamic_slice.13
  1.6 0.7 reduce_sum.49
  2.3 1.0 %fusion.6 = f32[12]{0:T(128)S(1)} fusion(bf16[12,2048]{1,0:T(8,128)(2,1)} %param.20), kind=kLoop, calls=%fused_computation.13 | loop fusion | flops 73716 | bytes 49200 | tf_op jit(solution)/shard_map/reduce_sum | solution.py:18
  3.3 1.1 %fusion.10 = f32[12,2]{0,1:T(2,128)S(1)} fusion(bf16[2048,4]{0,1:T(4,128)(2,1)} %param.26, s32[]{:T(128)S(6)} %select_n.18, bf16[12,2048]{1,0:T(8,128)(2,1)} %param.20, f32[2048]{0:T(1024)} %param.21, f32[12]{0:T(128)S(1)} %add_rsqrt_fusion.1), kind=kOutput, calls=%fused_computation.31 | convolution fusion | flops 196608 | bytes 82068 | tf_op jit(solution)/shard_map/dot_general | solution.py:362
  4.4 1.1 %subtract_exponential_fusion.1 = (f32[12,2]{0,1:T(2,128)S(1)}, f32[12,2]{0,1:T(2,128)S(1)}) fusion(f32[12,2]{0,1:T(2,128)S(1)} %fusion.10, f32[12,2]{0,1:T(2,128)} %param.33, f32[2]{0:T(128)S(1)} %dynamic_slice.13, bf16[2048,4]{0,1:T(4,128)(2,1)} %param.27, s32[]{:T(128)S(6)} %select_n.18, bf16[12,2048]{1,0:T(8,128)(2,1)} %param.20, f32[2048]{0:T(1024)} %param.21, ...), kind=kOutput, calls=%fused_computation.42 | convolution fusion | flops 196896 | bytes 83292 | tf_op jit(solution)/shard_map/dot_general | solution.py:364
  5.5 0.8 dynamic_slice.15
  6.3 0.1 mul.158
  6.5 0.1 copy.52
  6.6 0.1 copy.53
  6.7 0.8 copy.57
  7.5 1.7 %convert_reduce_fusion = s32[12,4]{1,0:T(8,128)S(1)} fusion(s32[12,4]{0,1:T(4,128)} %param.35, s32[12,4]{1,0:T(8,128)S(1)} %copy.57, pred[12,12]{1,0:T(8,128)(4,1)S(1)} %iota_compare_fusion.2), kind=kLoop, calls=%fused_computation.16 | loop fusion | flops 9168 | bytes 720 | tf_op jit(solution)/shard_map/reduce_sum | solution.py:308
  9.2 0.1 copy.64
  9.3 0.8 copy.59
  10.2 1.8 %fusion.26 = f32[12,384]{1,0:T(8,128)S(1)} fusion(bf16[2048,384]{1,0:T(8,128)(2,1)} %param.22, bf16[12,2048]{1,0:T(8,128)(2,1)} %param.20, f32[2048]{0:T(1024)} %param.21, f32[12]{0:T(128)S(1)} %add_rsqrt_fusion.1), kind=kOutput, calls=%fused_computation.48 | convolution fusion | flops 18972672 | bytes 1648688 | tf_op jit(solution)/shard_map/dot_general | solution.py:350
  12.0 0.1 reshape.82
  12.2 0.3 convolution_multiply_fusion
  12.6 0.1 broadcast_in_dim_reshape.2
  12.7 0.7 multiply_reduce_fusion.1
  13.4 0.1 copy.55
  13.5 0.1 copy.56
  13.6 1.8 %fusion.21 = f32[12,384]{1,0:T(8,128)S(1)} fusion(bf16[2048,384]{1,0:T(8,128)(2,1)} %param.24, bf16[12,2048]{1,0:T(8,128)(2,1)S(1)} %copy-done.5, f32[2048]{0:T(1024)S(1)} %copy-done.7, f32[12]{0:T(128)S(1)} %add_rsqrt_fusion.1), kind=kOutput, calls=%fused_computation.47 | convolution fusion | flops 18972672 | bytes 1648688 | tf_op jit(solution)/shard_map/dot_general | solution.py:352
  15.4 0.1 mul.148
  15.6 2.8 %multiply_add_fusion = f32[12,2,192,192]{3,2,1,0:T(8,128)S(1)} fusion(f32[12,2,192,192]{3,2,1,0:T(8,128)} %param.31, f32[12,2,192]{2,1,0:T(2,128)S(1)} %mul.148, f32[12,2,192]{2,1,0:T(2,128)S(1)} %get-tuple-element.8, f32[12,2]{1,0:T(8,128)S(1)} %copy.52), kind=kLoop, calls=%fused_computation | loop fusion | flops 2654208 | bytes 7114848 | tf_op jit(solution)/shard_map/add | solution.py:370
  18.4 0.4 fusion.28
  18.8 1.7 %copy-done.4 = f32[12,2,192,192]{3,2,1,0:T(8,128)} copy-done((f32[12,2,192,192]{3,2,1,0:T(8,128)}, f32[12,2,192,192]{3,2,1,0:T(8,128)S(1)}, u32[]{:S(2)}) %copy-start.4) | copy-done | bytes 3538968
  20.6 0.2 multiply_reduce_fusion
  20.9 0.1 reshape.77
  21.0 1.9 %fusion.4 = bf16[12,384]{1,0:T(8,128)(2,1)S(1)} fusion(f32[12,384]{1,0:T(8,128)S(1)} %reshape.77, bf16[2048,384]{1,0:T(8,128)(2,1)} %param.25, bf16[12,2048]{1,0:T(8,128)(2,1)S(1)} %copy-done.5, f32[2048]{0:T(1024)S(1)} %copy-done.7, f32[12]{0:T(128)S(1)} %add_rsqrt_fusion.1), kind=kOutput, calls=%fused_computation.8 | convolution fusion | flops 18995712 | bytes 1657904 | tf_op jit(solution)/shard_map/dot_general | solution.py:353
  22.9 0.3 convolution_convert_fusion.part_ref
  23.2 1.6 %copy-done.2 = bf16[1,2048,512]{2,1,0:T(8,128)(2,1)S(1)} copy-done((bf16[1,2048,512]{2,1,0:T(8,128)(2,1)S(1)}, bf16[1,2048,512]{2,1,0:T(8,128)(2,1)}, u32[]{:S(2)}) %copy-start.2) | copy-done | bytes 2097176
  24.8 68.7 %experts.1 = bf16[12,2048]{1,0:T(8,128)(2,1)S(1)} custom-call(bf16[16,2048]{1,0:T(8,128)(2,1)S(1)} %convolution_convert_fusion.part_ref, bf16[16,2048]{1,0:T(8,128)(2,1)S(1)} %pad.17.tok_ref, f32[1,2048]{1,0:T(1,128)S(1)} %bitcast.17, f32[24,128]{1,0:T(8,128)S(1)} %pad_maximum_fusion.meta_ref, bf16[2048,512]{1,0:T(8,128)(2,1)S(1)} %bitcast.15, ...), custom_call_target="tpu_custom_call" | custom-call | tf_op jit(solution)/shard_map/experts/pallas_call | solution.py:269
  93.6 0.6 copy.68
  (37 shorter events, 0.7 us)
Async XLA Ops:
  0.6 22.3 %copy-start = (bf16[384,2048]{1,0:T(8,128)(2,1)S(1)}, bf16[384,2048]{1,0:T(8,128)(2,1)}, u32[]{:S(2)}) copy-start(bf16[384,2048]{1,0:T(8,128)(2,1)} %param.30) | copy-start | bytes 4718596
  0.6 11.6 %copy-start.5 = (bf16[12,2048]{1,0:T(8,128)(2,1)S(1)}, bf16[12,2048]{1,0:T(8,128)(2,1)}, u32[]{:S(2)}) copy-start(bf16[12,2048]{1,0:T(8,128)(2,1)} %param.20) | copy-start | bytes 147460
  0.7 11.6 %copy-start.7 = (f32[2048]{0:T(1024)S(1)}, f32[2048]{0:T(1024)}, u32[]{:S(2)}) copy-start(f32[2048]{0:T(1024)} %param.21) | copy-start | bytes 24580
  0.7 11.6 %copy-start.6 = (bf16[2048,384]{1,0:T(8,128)(2,1)S(1)}, bf16[2048,384]{1,0:T(8,128)(2,1)}, u32[]{:S(2)}) copy-start(bf16[2048,384]{1,0:T(8,128)(2,1)} %param.23) | copy-start | bytes 4718596
  5.5 8.0 %copy-start.9 = (f32[12,2]{0,1:T(2,128)}, f32[12,2]{0,1:T(2,128)S(1)}, u32[]{:S(2)}) copy-start(f32[12,2]{0,1:T(2,128)S(1)} %get-tuple-element.18) | copy-start | bytes 292
  10.2 2.5 %copy-start.8 = (f32[12,2,192]{2,1,0:T(2,128)S(1)}, f32[12,2,192]{2,1,0:T(2,128)}, u32[]{:S(2)}) copy-start(f32[12,2,192]{2,1,0:T(2,128)} %param.32) | copy-start | bytes 55300
  18.4 2.2 %copy-start.4 = (f32[12,2,192,192]{3,2,1,0:T(8,128)}, f32[12,2,192,192]{3,2,1,0:T(8,128)S(1)}, u32[]{:S(2)}) copy-start(f32[12,2,192,192]{3,2,1,0:T(8,128)S(1)} %multiply_add_fusion) | copy-start | bytes 10616836
  20.9 2.3 %copy-start.1 = (bf16[1,2048,512]{2,1,0:T(8,128)(2,1)S(1)}, bf16[1,2048,512]{2,1,0:T(8,128)(2,1)}, u32[]{:S(2)}) copy-start(bf16[1,2048,512]{2,1,0:T(8,128)(2,1)} %param.37) | copy-start | bytes 6291460
  20.9 2.3 %copy-start.3 = (f32[2048]{0:T(1024)S(1)}, f32[2048]{0:T(1024)}, u32[]{:S(2)}) copy-start(f32[2048]{0:T(1024)} %param.34) | copy-start | bytes 24580
  23.2 1.6 %copy-start.2 = (bf16[1,2048,512]{2,1,0:T(8,128)(2,1)S(1)}, bf16[1,2048,512]{2,1,0:T(8,128)(2,1)}, u32[]{:S(2)}) copy-start(bf16[1,2048,512]{2,1,0:T(8,128)(2,1)} %param.38) | copy-start | bytes 6291460

commit v2 on v1

v2 whole, which is shorter than its diff:
```python
import functools

import jax
import jax.numpy as jnp
from jax import lax
from jax.experimental import pallas as pl
from jax.experimental.pallas import tpu as pltpu
from jax.sharding import PartitionSpec as P

EPS = 1e-06
PLANE = 16
FULL_VMEM = 67043328
BF16 = jnp.bfloat16
F32 = jnp.float32


def rms_scaled(values, scales):
    floats = values.astype(F32)
    return floats * lax.rsqrt(jnp.mean(floats * floats, axis=-1, keepdims=True) + EPS) * scales


def place_of(d, nz):
    if d == 0:
        return 0
    return 2 * d - 1 if d <= nz // 2 else 2 * (nz - d)


def moe_kernel(
    nz,
    ng,
    gated_ref,
    meta_ref,
    wout_hbm,
    tok_hbm,
    gain_hbm,
    wg_hbm,
    wu_hbm,
    wd_hbm,
    out_ref,
    wout,
    tok_ref,
    gain_ref,
    wg,
    wu,
    wd,
    pbuf,
    meta,
    zrows,
    snd,
    rcv,
    osnd,
    back,
    zsnd,
    zrcv,
    hbuf,
    w_sem,
    p_sem,
    m_sem,
    z_sem,
    d_sem,
    b_sem,
    r_sem,
    f_sem,
):
    ep = lax.axis_index("ep")
    tp = lax.axis_index("tp")
    z = ep // ng
    g = ep % ng
    me = g * 2 + tp
    other = 1 - tp
    np_ = 2 * ng
    count, width = tok_ref.shape
    rows, half = zrows.shape[1:]
    per = nz // 2
    slots = 2 * per

    copies = [
        pltpu.make_async_copy(src, dst, w_sem.at[i])
        for i, (src, dst) in enumerate(
            (
                (wout_hbm, wout),
                (tok_hbm, tok_ref),
                (gain_hbm, gain_ref),
                (wg_hbm, wg),
                (wu_hbm, wu),
                (wd_hbm, wd),
            )
        )
    ]
    weights = copies[3:]
    for copy in copies:
        copy.start()

    barrier = pltpu.get_barrier_semaphore()

    @pl.loop(1, nz)
    def _(d):
        pl.semaphore_signal(barrier, inc=1, device_id=(lax.rem(z + d, nz) * ng + g, tp))

    @pl.loop(1, np_)
    def _(d):
        q = lax.rem(me + d, np_)
        pl.semaphore_signal(barrier, inc=1, device_id=(z * ng + q // 2, q % 2))

    copies[0].wait()
    pbuf[0] = jnp.dot(gated_ref[...], wout[...], preferred_element_type=F32).astype(BF16)
    meta[0] = meta_ref[...]
    pl.semaphore_wait(barrier, nz - 1 + np_ - 1)

    def remote(src, dst, sems, at_src, at_dst, to_ep, to_tp):
        return pltpu.make_async_remote_copy(
            src_ref=src,
            dst_ref=dst,
            send_sem=sems.at[0, at_src],
            recv_sem=sems.at[1, at_dst],
            device_id=(to_ep, to_tp),
        )

    def along_z(sems, source, target):
        sent, arriving = {}, {}
        for d in range(1, nz):
            there, here = place_of(nz - d, nz), place_of(d, nz)
            to = lax.rem(z + d, nz) * ng + g
            sent[here] = remote(source(here), target(there), sems, here, there, to, tp)
            arriving[here] = remote(source(here), target(here), sems, here, here, to, tp)
        return sent, arriving

    swap = remote(pbuf.at[0], pbuf.at[1], p_sem, 0, 0, ep, other)
    swap.start()
    meta_out, meta_in = along_z(m_sem, lambda o: meta.at[0], lambda o: meta.at[o])
    for o in range(1, nz):
        meta_out[o].start()

    copies[1].wait()
    copies[2].wait()
    swap.wait_recv()
    mixed = (pbuf[0].astype(F32) + pbuf[1].astype(F32)).astype(BF16)
    resid = (tok_ref[...].astype(F32) + mixed.astype(F32)).astype(BF16)
    ffn_in = rms_scaled(resid, gain_ref[...]).astype(BF16)

    def my_half(values):
        return jnp.where(tp == 0, values[:, :half], values[:, half:])

    if rows > count:
        zrows[0] = jnp.zeros((rows, half), BF16)
    zrows[0, :count, :] = my_half(ffn_in)
    z_out, z_in = along_z(z_sem, lambda o: zrows.at[0], lambda o: zrows.at[o])
    for o in range(1, nz):
        z_out[o].start()

    for o in range(1, nz):
        meta_in[o].wait_recv()

    first = (z * ng + 1).astype(F32)
    lanes = per * rows
    picks, mixes = [], []
    for c in range(2):
        whole = [
            meta[c * per + i, rows:, :] if i == 0 else pltpu.roll(meta[c * per + i, rows:, :], i * rows, 1)
            for i in range(per)
        ]
        by_lane = whole[0]
        for part in whole[1:]:
            by_lane = by_lane + part
        source = lax.broadcasted_iota(jnp.int32, (4, lanes), 1) // rows
        slot_t = (
            (by_lane[0:4, :lanes] - first) * slots + by_lane[4:8, :lanes]
        ).astype(jnp.int32) + 2 * source
        slot_at = lax.broadcasted_iota(jnp.int32, (ng * slots, lanes), 0)
        pick = jnp.zeros((ng * slots, lanes), F32)
        for k in range(4):
            pick = pick + jnp.where(slot_at == slot_t[k : k + 1, :], 1.0, 0.0)
        picks.append(pick.astype(BF16))
        by_row = meta[c * per : (c + 1) * per, :rows, :].reshape(lanes, meta.shape[2])
        source = lax.broadcasted_iota(jnp.int32, (lanes, 4), 0) // rows
        slot_r = ((by_row[:, 0:4] - first) * slots + by_row[:, 8:12]).astype(jnp.int32) + 2 * source
        slot_at = lax.broadcasted_iota(jnp.int32, (lanes, ng * slots), 1)
        mix = jnp.zeros((lanes, ng * slots), F32)
        for k in range(4):
            mix = mix + jnp.where(slot_at == slot_r[:, k : k + 1], by_row[:, 4 + k : 5 + k], 0.0)
        mix_hi = mix.astype(BF16)
        mixes.append((mix_hi, (mix - mix_hi.astype(F32)).astype(BF16)))

    def d_copy(c, d, at):
        q = lax.rem(me + d, np_)
        to_g, to_tp = q // 2, q % 2
        return remote(
            snd.at[c, to_g],
            rcv.at[c, at % 2, at // 2],
            d_sem.at[c],
            d,
            at,
            z * ng + to_g,
            to_tp,
        )

    for c in range(2):
        for o in range(max(1, c * per), (c + 1) * per):
            z_in[o].wait_recv()
        gathered = zrows[c * per : (c + 1) * per].reshape(lanes, half)
        snd[c] = (
            jnp.dot(picks[c], gathered, preferred_element_type=F32)
            .astype(BF16)
            .reshape(ng, slots, half)
        )

        @pl.loop(1, np_)
        def _(d):
            d_copy(c, d, me).start()

        rcv[c, tp, g] = snd[c, g]

    for copy in weights:
        copy.wait()

    def b_copy(c, d, at):
        q = lax.rem(me + d, np_)
        to_g, to_tp = q // 2, q % 2
        return remote(
            osnd.at[c, to_tp, to_g],
            back.at[c, at % 2, at // 2],
            b_sem.at[c],
            d,
            at,
            z * ng + to_g,
            to_tp,
        )

    for c in range(2):

        @pl.loop(1, np_)
        def _(d):
            d_copy(c, d, lax.rem(me + d, np_)).wait_recv()

        left = rcv[c, 0].reshape(ng * slots, half)
        right = rcv[c, 1].reshape(ng * slots, half)

        def both(w):
            return jnp.dot(left, w[:half, :], preferred_element_type=F32) + jnp.dot(
                right, w[half:, :], preferred_element_type=F32
            )

        gate_val = both(wg)
        hidden = (gate_val * jax.nn.sigmoid(gate_val) * both(wu)).astype(BF16)
        for h in range(2):
            osnd[c, h] = (
                jnp.dot(hidden, wd[:, h * half : (h + 1) * half], preferred_element_type=F32)
                .astype(BF16)
                .reshape(ng, slots, half)
            )

        @pl.loop(1, np_)
        def _(d):
            b_copy(c, d, me).start()

        back[c, tp, g] = osnd[c, tp, g]

    r_out, r_in = along_z(r_sem, lambda o: zsnd.at[o], lambda o: zrcv.at[o])
    for c in range(2):

        @pl.loop(1, np_)
        def _(d):
            b_copy(c, d, lax.rem(me + d, np_)).wait_recv()

        served = (
            (back[c, 0].astype(F32) + back[c, 1].astype(F32)).astype(BF16).reshape(ng * slots, half)
        )
        mix_hi, mix_lo = mixes[c]
        sums = jnp.dot(mix_hi, served, preferred_element_type=F32) + jnp.dot(
            mix_lo, served, preferred_element_type=F32
        )
        zsnd[c * per : (c + 1) * per] = sums.astype(BF16).reshape(per, rows, half)
        for o in range(max(1, c * per), (c + 1) * per):
            r_out[o].start()

    total = my_half(resid).astype(F32) + zsnd[0, :count, :].astype(F32)
    for o in range(1, nz):
        r_in[o].wait_recv()
        total = total + zrcv[o, :count, :].astype(F32)
    mine = total.astype(BF16)
    hbuf[0] = mine
    last = remote(hbuf.at[0], hbuf.at[1], f_sem, 0, 0, ep, other)
    last.start()
    last.wait_recv()
    theirs = hbuf[1]
    out_ref[:, :half] = jnp.where(tp == 0, mine, theirs)
    out_ref[:, half:] = jnp.where(tp == 0, theirs, mine)

    swap.wait_send()
    last.wait_send()
    for o in range(1, nz):
        meta_out[o].wait_send()
        z_out[o].wait_send()
        r_out[o].wait_send()
    for c in range(2):

        @pl.loop(1, np_)
        def _(d):
            d_copy(c, d, me).wait_send()
            b_copy(c, d, me).wait_send()


def moe(nz, ng, gated, meta, wout, tok, gain, wg, wu, wd):
    count, width = tok.shape
    rows = meta.shape[0] - 8
    half = width // 2
    vmem = pl.BlockSpec(memory_space=pltpu.VMEM)
    hbm = pl.BlockSpec(memory_space=pltpu.HBM)

    def sems(*n):
        return pltpu.SemaphoreType.DMA(n)

    return pl.pallas_call(
        functools.partial(moe_kernel, nz, ng),
        out_shape=jax.ShapeDtypeStruct((count, width), BF16),
        in_specs=[vmem] * 2 + [hbm] * 6,
        out_specs=vmem,
        scratch_shapes=[pltpu.VMEM(a.shape, a.dtype) for a in (wout, tok, gain, wg, wu, wd)]
        + [
            pltpu.VMEM((2, count, width), BF16),
            pltpu.VMEM((nz, *meta.shape), F32),
            pltpu.VMEM((nz, rows, half), BF16),
            pltpu.VMEM((2, ng, nz, half), BF16),
            pltpu.VMEM((2, 2, ng, nz, half), BF16),
            pltpu.VMEM((2, 2, ng, nz, half), BF16),
            pltpu.VMEM((2, 2, ng, nz, half), BF16),
            pltpu.VMEM((nz, rows, half), BF16),
            pltpu.VMEM((nz, rows, half), BF16),
            pltpu.VMEM((2, count, half), BF16),
            sems(6),
            sems(2, 1),
            sems(2, nz),
            sems(2, nz),
            sems(2, 2, 2 * ng),
            sems(2, 2, 2 * ng),
            sems(2, nz),
            sems(2, 1),
        ],
        compiler_params=pltpu.CompilerParams(
            collective_id=0, has_side_effects=True, vmem_limit_bytes=FULL_VMEM
        ),
        name="experts",
    )(gated, meta, wout, tok, gain, wg, wu, wd)


def cell_kernel(
    tok_hbm,
    ngain_hbm,
    wi_hbm,
    wf_hbm,
    bias_hbm,
    hgain_hbm,
    norm_hbm,
    stab_hbm,
    ids_hbm,
    probs_hbm,
    wq_hbm,
    wk_hbm,
    wv_hbm,
    wo_hbm,
    mem_hbm,
    gated_ref,
    meta_ref,
    nnorm_ref,
    nstab_ref,
    nmem_hbm,
    tok_ref,
    ngain_ref,
    wi_ref,
    wf_ref,
    bias_ref,
    hgain_ref,
    norm_ref,
    stab_ref,
    ids_ref,
    probs_ref,
    wq,
    wk,
    wv,
    wo,
    mem,
    num,
    s_sem,
    w_sem,
    in_sem,
    out_sem,
):
    tp = lax.axis_index("tp")
    count, width = tok_ref.shape
    heads, dim = norm_ref.shape[1:]
    small = [
        pltpu.make_async_copy(src, dst, s_sem.at[i])
        for i, (src, dst) in enumerate(
            (
                (ids_hbm, ids_ref),
                (probs_hbm, probs_ref),
                (tok_hbm, tok_ref),
                (ngain_hbm, ngain_ref),
                (wi_hbm, wi_ref),
                (wf_hbm, wf_ref),
                (bias_hbm, bias_ref),
                (stab_hbm, stab_ref),
                (norm_hbm, norm_ref),
                (hgain_hbm, hgain_ref),
            )
        )
    ]
    loads = [
        pltpu.make_async_copy(src, dst, w_sem.at[i])
        for i, (src, dst) in enumerate(
            ((wk_hbm, wk), (wv_hbm, wv), (wq_hbm, wq), (wo_hbm, wo))
        )
    ]
    reads = [pltpu.make_async_copy(mem_hbm.at[b], mem.at[b], in_sem.at[b]) for b in range(count)]
    writes = [pltpu.make_async_copy(mem.at[b], nmem_hbm.at[b], out_sem.at[b]) for b in range(count)]
    for copy in small + loads + reads:
        copy.start()

    for copy in small:
        copy.wait()
    ids = ids_ref[...].astype(F32).T.astype(jnp.int32)
    probs = probs_ref[...].T
    weights = probs / jnp.sum(probs, axis=-1, keepdims=True)
    lane = lax.broadcasted_iota(jnp.int32, (count, 128), 1)
    row = lax.broadcasted_iota(jnp.int32, (count, 128), 0)
    top = ids.shape[1]
    named = [lane == ids[:, k : k + 1] for k in range(top)]
    onehot = jnp.zeros((count, 128), F32)
    for k in range(top):
        onehot = onehot + jnp.where(named[k], 1.0, 0.0)
    rows16 = meta_ref.shape[0] - 8
    lower = lax.broadcasted_iota(jnp.int32, (count, count), 0) > lax.broadcasted_iota(
        jnp.int32, (count, count), 1
    )
    earlier = jnp.dot(
        jnp.where(lower, 1.0, 0.0).astype(BF16), onehot.astype(BF16), preferred_element_type=F32
    )
    by_row = jnp.zeros((count, 128), F32)
    meta_ref[...] = jnp.zeros(meta_ref.shape, F32)
    for k in range(top):
        rank = jnp.sum(jnp.where(named[k], earlier, 0.0), axis=1, keepdims=True)
        code = ids[:, k : k + 1].astype(F32) + 1.0
        for at, what in ((k, code), (4 + k, weights[:, k : k + 1]), (8 + k, rank)):
            by_row = jnp.where(lane == at, what, by_row)
        for at, what in ((k, code), (4 + k, rank)):
            meta_ref[rows16 + at : rows16 + at + 1, :] = jnp.sum(
                jnp.where(lane == row, what, 0.0), axis=0, keepdims=True
            )
    meta_ref[:count, :] = by_row

    normed = rms_scaled(tok_ref[...], ngain_ref[...]).astype(BF16)
    across = (((1,), (1,)), ((), ()))
    pre_all = lax.dot_general(normed, wi_ref[...], across, preferred_element_type=F32)
    forget_all = jax.nn.log_sigmoid(
        lax.dot_general(normed, wf_ref[...], across, preferred_element_type=F32) + bias_ref[...]
    )

    def project(i, w):
        loads[i].wait()
        return jnp.dot(normed, w[...], preferred_element_type=F32)

    key = project(0, wk) * dim ** (-0.5)
    value = project(1, wv)
    query = project(2, wq)
    outgate = project(3, wo)
    query_t = query.T
    stab = stab_ref[...].T
    new_stabs = []
    keeps, values, keys_t, floors = [], [], [], []
    for h in range(heads):
        pre = jnp.where(tp == 0, pre_all[:, h : h + 1], pre_all[:, heads + h : heads + h + 1])
        forget = jnp.where(
            tp == 0, forget_all[:, h : h + 1], forget_all[:, heads + h : heads + h + 1]
        )
        carried = forget + stab[:, h : h + 1]
        new_stab = jnp.maximum(carried, pre)
        new_stabs.append(new_stab)
        keep = jnp.exp(carried - new_stab)
        at = slice(h * dim, (h + 1) * dim)
        written = jnp.exp(pre - new_stab) * key[:, at]
        new_norm = keep * norm_ref[:, h, :] + written
        nnorm_ref[:, h, :] = new_norm
        den = jnp.sum(query[:, at] * new_norm, axis=1, keepdims=True)
        floors.append(jnp.maximum(jnp.abs(den), jnp.exp(-new_stab)))
        keeps.append(jnp.broadcast_to(keep, (count, dim)))
        values.append(value[:, at])
        keys_t.append(written.T)
    heads_at = lax.broadcasted_iota(jnp.int32, (count, heads), 1)
    both_stabs = jnp.broadcast_to(new_stabs[0], (count, heads))
    for h in range(1, heads):
        both_stabs = jnp.where(heads_at == h, new_stabs[h], both_stabs)
    nstab_ref[...] = both_stabs.T
    for b in range(count):
        reads[b].wait()
        for h in range(heads):
            new = keeps[h][b : b + 1, :] * mem[b, h] + (
                keys_t[h][:, b : b + 1] * values[h][b : b + 1, :]
            )
            mem[b, h] = new
            num[h, b : b + 1, :] = jnp.sum(
                query_t[h * dim : (h + 1) * dim, b : b + 1] * new, axis=0, keepdims=True
            )
        writes[b].start()
    local_width = heads * dim
    parts = local_width // 128
    gains = jnp.concatenate(
        [
            jnp.where(tp == 0, hgain_ref[i : i + 1, :], hgain_ref[parts + i : parts + i + 1, :])
            for i in range(parts)
        ],
        axis=1,
    )
    for h in range(heads):
        at = slice(h * dim, (h + 1) * dim)
        readout = num[h] / floors[h]
        scaled = (
            readout
            * lax.rsqrt(jnp.mean(readout * readout, axis=-1, keepdims=True) + EPS)
            * gains[:, at]
        )
        gated_ref[:, at] = (scaled * jax.nn.sigmoid(outgate[:, at])).astype(BF16)
    for copy in writes:
        copy.wait()


def cell(small, weights, memory):
    count, width = small[0].shape
    rows16 = -(-count // 16) * 16
    norm_shape = small[6].shape
    vmem = pl.BlockSpec(memory_space=pltpu.VMEM)
    hbm = pl.BlockSpec(memory_space=pltpu.HBM)
    return pl.pallas_call(
        cell_kernel,
        out_shape=(
            jax.ShapeDtypeStruct((count, weights[0].shape[1]), BF16),
            jax.ShapeDtypeStruct((rows16 + 8, 128), F32),
            jax.ShapeDtypeStruct(norm_shape, F32),
            jax.ShapeDtypeStruct((norm_shape[1], count), F32),
            jax.ShapeDtypeStruct(memory.shape, F32),
        ),
        in_specs=[hbm] * (len(small) + len(weights) + 1),
        out_specs=(vmem, vmem, vmem, vmem, hbm),
        scratch_shapes=[pltpu.VMEM(a.shape, a.dtype) for a in (*small, *weights, memory)]
        + [
            pltpu.VMEM((norm_shape[1], count, norm_shape[2]), F32),
            pltpu.SemaphoreType.DMA((len(small),)),
            pltpu.SemaphoreType.DMA((len(weights),)),
            pltpu.SemaphoreType.DMA((count,)),
            pltpu.SemaphoreType.DMA((count,)),
        ],
        compiler_params=pltpu.CompilerParams(vmem_limit_bytes=FULL_VMEM),
        name="cell",
    )(*small, *weights, memory)


def local(
    tokens,
    norm_gain,
    w_query,
    w_key,
    w_value,
    w_outgate,
    w_input_gate,
    w_forget_gate,
    forget_bias,
    head_gain,
    w_output,
    memory,
    normalizer,
    stabilizer,
    ffn_gain,
    route_ids,
    route_probs,
    expert_gate,
    expert_up,
    expert_down,
):
    ep_count = lax.axis_size("ep")
    ng = min(PLANE, ep_count // 2)
    nz = ep_count // ng
    gated, meta, new_normalizer, new_stab, new_memory = cell(
        (
            tokens,
            norm_gain.reshape(1, -1),
            w_input_gate.T,
            w_forget_gate.T,
            forget_bias.reshape(1, -1),
            head_gain.reshape(-1, 128),
            normalizer,
            stabilizer.T,
            route_ids.T,
            route_probs.T,
        ),
        (w_query, w_key, w_value, w_outgate),
        memory,
    )
    next_tokens = moe(
        nz,
        ng,
        gated,
        meta,
        w_output,
        tokens,
        ffn_gain.reshape(1, -1),
        expert_gate[0],
        expert_up[0],
        expert_down[0],
    )
    return (next_tokens, new_memory, new_normalizer, new_stab.T)


def solution(mesh):
    return jax.shard_map(
        local,
        mesh=mesh,
        in_specs=(
            P("ep", None),
            P(),
            P(None, "tp"),
            P(None, "tp"),
            P(None, "tp"),
            P(None, "tp"),
            P(),
            P(),
            P(),
            P(),
            P("tp", None),
            P("ep", "tp", None, None),
            P("ep", "tp", None),
            P("ep", "tp"),
            P(),
            P("ep", None),
            P("ep", None),
            P("ep", None, "tp"),
            P("ep", None, "tp"),
            P("ep", "tp", None),
        ),
        out_specs=(P("ep", None), P("ep", "tp", None, None), P("ep", "tp", None), P("ep", "tp")),
        check_vma=False,
    )
```

time: 94.7 us -> 72.6 us (0.77)
  the two profiles are of different devices: /device:TPU:4 before, /device:TPU:36 now
where the time goes in v2:
time: 72.6 us; the launch traced here: 72.4 us
  Pallas kernels  70.3 us (97%)
  local copies, waits for them, and re-layouts  1.47 us (2%)
    pallas_call x1, Pallas kernels, moe(): pl.pallas_call(functools.partial(moe_kernel, nz, ng), out_shape=jax.Shape...  59.5 us
    pallas_call x1, Pallas kernels, cell(): pl.pallas_call(cell_kernel, out_shape=(jax.ShapeDtypeStruct((count, weigh...  10.8 us
    unnamed x1, local copies, waits for them, and re-layouts  1.47 us

profile of v2, /device:TPU:36, one launch (start us, length us, event | category | flops | bytes accessed | tf_op | source)
XLA Modules:
  0.0 72.4 jit_solution(16277075259927673557)
XLA Ops:
  0.6 10.8 %cell.1 = (bf16[12,384]{1,0:T(8,128)(2,1)}, f32[24,128]{1,0:T(8,128)}, f32[12,2,192]{2,1,0:T(2,128)}, f32[2,12]{1,0:T(2,128)}, f32[12,2,192,192]{3,2,1,0:T(8,128)}) custom-call(bf16[12,2048]{1,0:T(8,128)(2,1)} %tok_hbm.3, f32[1,2048]{1,0:T(1,128)} %bitcast.18, bf16[4,2048]{1,0:T(4,128)(2,1)} %bitcast.16, bf16[4,2048]{1,0:T(4,128)(2,1)} %bitcast.17, ...), custom_call_target="tpu_custom_call" | custom-call | tf_op jit(solution)/shard_map/cell/pallas_call | solution.py:532
  11.4 59.5 %experts.1 = bf16[12,2048]{1,0:T(8,128)(2,1)} custom-call(bf16[12,384]{1,0:T(8,128)(2,1)} %get-tuple-element.9.gated_ref, f32[24,128]{1,0:T(8,128)} %get-tuple-element.10.meta_ref, bf16[384,2048]{1,0:T(8,128)(2,1)} %wout_hbm.1, bf16[12,2048]{1,0:T(8,128)(2,1)} %tok_hbm.3, f32[1,2048]{1,0:T(1,128)} %bitcast.19, bf16[2048,512]{1,0:T(8,128)(2,1)} %bitcast.13, ...), custom_call_target="tpu_custom_call" | custom-call | tf_op jit(solution)/shard_map/experts/pallas_call | solution.py:313
  70.9 1.5 %copy.25 = bf16[12,2048]{1,0:T(8,128)(2,1)} copy(bf16[12,2048]{1,0:T(8,128)(2,1)} %experts.1) | data formatting | bytes 98304

commit v3 on v2

--- a/solution.py
+++ b/solution.py
@@ -28,8 +28,8 @@
 def moe_kernel(
     nz,
     ng,
-    gated_ref,
-    meta_ref,
+    gated_hbm,
+    meta_hbm,
     wout_hbm,
     tok_hbm,
     gain_hbm,
@@ -37,6 +37,7 @@
     wu_hbm,
     wd_hbm,
     out_ref,
+    gated_ref,
     wout,
     tok_ref,
     gain_ref,
@@ -48,10 +49,18 @@
     zrows,
     snd,
     rcv,
-    osnd,
-    back,
-    zsnd,
-    zrcv,
+    osnd0,
+    osnd1,
+    osnd2,
+    back0,
+    back1,
+    back2,
+    zsnd0,
+    zsnd1,
+    zsnd2,
+    zrcv0,
+    zrcv1,
+    zrcv2,
     hbuf,
     w_sem,
     p_sem,
@@ -78,7 +87,9 @@
         pltpu.make_async_copy(src, dst, w_sem.at[i])
         for i, (src, dst) in enumerate(
             (
+                (gated_hbm, gated_ref),
                 (wout_hbm, wout),
+                (meta_hbm, meta.at[0]),
                 (tok_hbm, tok_ref),
                 (gain_hbm, gain_ref),
                 (wg_hbm, wg),
@@ -87,8 +98,8 @@
             )
         )
     ]
-    weights = copies[3:]
-    for copy in copies:
+    weights = copies[5:]
+    for copy in copies[:5]:
         copy.start()
 
     barrier = pltpu.get_barrier_semaphore()
@@ -103,8 +114,12 @@
         pl.semaphore_signal(barrier, inc=1, device_id=(z * ng + q // 2, q % 2))
 
     copies[0].wait()
+    copies[1].wait()
+    for copy in weights:
+        copy.start()
     pbuf[0] = jnp.dot(gated_ref[...], wout[...], preferred_element_type=F32).astype(BF16)
-    meta[0] = meta_ref[...]
+    for copy in copies[2:5]:
+        copy.wait()
     pl.semaphore_wait(barrier, nz - 1 + np_ - 1)
 
     def remote(src, dst, sems, at_src, at_dst, to_ep, to_tp):
@@ -116,10 +131,11 @@
             device_id=(to_ep, to_tp),
         )
 
-    def along_z(sems, source, target):
+    def along_z(sems, source, target, places=range(1, nz)):
         sent, arriving = {}, {}
-        for d in range(1, nz):
-            there, here = place_of(nz - d, nz), place_of(d, nz)
+        for here in places:
+            d = [d for d in range(nz) if place_of(d, nz) == here][0]
+            there = place_of(nz - d, nz)
             to = lax.rem(z + d, nz) * ng + g
             sent[here] = remote(source(here), target(there), sems, here, there, to, tp)
             arriving[here] = remote(source(here), target(here), sems, here, here, to, tp)
@@ -131,8 +147,6 @@
     for o in range(1, nz):
         meta_out[o].start()
 
-    copies[1].wait()
-    copies[2].wait()
     swap.wait_recv()
     mixed = (pbuf[0].astype(F32) + pbuf[1].astype(F32)).astype(BF16)
     resid = (tok_ref[...].astype(F32) + mixed.astype(F32)).astype(BF16)
@@ -213,13 +227,17 @@
     for copy in weights:
         copy.wait()
 
-    def b_copy(c, d, at):
+    osnd, back = (osnd0, osnd1, osnd2), (back0, back1, back2)
+    zsnd, zrcv = (zsnd0, zsnd1, zsnd2), (zrcv0, zrcv1, zrcv2)
+    units = [(0, 0, half), (1, 0, half // 2), (1, half // 2, half // 2)]
+
+    def b_copy(u, d, at):
         q = lax.rem(me + d, np_)
         to_g, to_tp = q // 2, q % 2
         return remote(
-            osnd.at[c, to_tp, to_g],
-            back.at[c, at % 2, at // 2],
-            b_sem.at[c],
+            osnd[u].at[to_tp, to_g],
+            back[u].at[at % 2, at // 2],
+            b_sem.at[u],
             d,
             at,
             z * ng + to_g,
@@ -242,41 +260,71 @@
 
         gate_val = both(wg)
         hidden = (gate_val * jax.nn.sigmoid(gate_val) * both(wu)).astype(BF16)
-        for h in range(2):
-            osnd[c, h] = (
-                jnp.dot(hidden, wd[:, h * half : (h + 1) * half], preferred_element_type=F32)
-                .astype(BF16)
-                .reshape(ng, slots, half)
-            )
+        for u, (chunk, start, size) in enumerate(units):
+            if chunk == c:
+                for h in range(2):
+                    cols = slice(h * half + start, h * half + start + size)
+                    osnd[u][h] = (
+                        jnp.dot(hidden, wd[:, cols], preferred_element_type=F32)
+                        .astype(BF16)
+                        .reshape(ng, slots, size)
+                    )
+
+                @pl.loop(1, np_)
+                def _(d):
+                    b_copy(u, d, me).start()
+
+                back[u][tp, g] = osnd[u][tp, g]
+
+    @pl.loop(1, np_)
+    def _(d):
+        for c in range(2):
+            d_copy(c, d, me).wait_send()
+
+    swap.wait_send()
+    for o in range(1, nz):
+        meta_out[o].wait_send()
+        z_out[o].wait_send()
+
+    summed = []
+    for u, (c, start, size) in enumerate(units):
+        r_out, _ = along_z(
+            r_sem.at[u],
+            lambda o: zsnd[u].at[o % per],
+            lambda o: zrcv[u].at[o],
+            range(max(1, c * per), (c + 1) * per),
+        )
 
         @pl.loop(1, np_)
         def _(d):
-            b_copy(c, d, me).start()
-
-        back[c, tp, g] = osnd[c, tp, g]
-
-    r_out, r_in = along_z(r_sem, lambda o: zsnd.at[o], lambda o: zrcv.at[o])
-    for c in range(2):
-
-        @pl.loop(1, np_)
-        def _(d):
-            b_copy(c, d, lax.rem(me + d, np_)).wait_recv()
-
-        served = (
-            (back[c, 0].astype(F32) + back[c, 1].astype(F32)).astype(BF16).reshape(ng * slots, half)
-        )
+            b_copy(u, d, lax.rem(me + d, np_)).wait_recv()
+
+        served = (back[u][0].astype(F32) + back[u][1].astype(F32)).astype(BF16)
+        served = served.reshape(ng * slots, size)
         mix_hi, mix_lo = mixes[c]
         sums = jnp.dot(mix_hi, served, preferred_element_type=F32) + jnp.dot(
             mix_lo, served, preferred_element_type=F32
         )
-        zsnd[c * per : (c + 1) * per] = sums.astype(BF16).reshape(per, rows, half)
-        for o in range(max(1, c * per), (c + 1) * per):
+        zsnd[u][...] = sums.astype(BF16).reshape(per, rows, size)
+        for o in r_out:
             r_out[o].start()
-
-    total = my_half(resid).astype(F32) + zsnd[0, :count, :].astype(F32)
-    for o in range(1, nz):
-        r_in[o].wait_recv()
-        total = total + zrcv[o, :count, :].astype(F32)
+            summed.append(r_out[o])
+
+    @pl.loop(1, np_)
+    def _(d):
+        for u in range(3):
+            b_copy(u, d, me).wait_send()
+
+    total = my_half(resid).astype(F32) + zsnd[0][0, :count, :].astype(F32)
+    for d in range(1, nz):
+        here, chunk = place_of(d, nz), place_of(nz - d, nz) // per
+        pieces = []
+        for u, (c, _, _) in enumerate(units):
+            if c == chunk:
+                at = zrcv[u].at[here]
+                remote(at, at, r_sem.at[u], here, here, ep, other).wait_recv()
+                pieces.append(zrcv[u][here, :count, :].astype(F32))
+        total = total + (pieces[0] if len(pieces) == 1 else jnp.concatenate(pieces, axis=1))
     mine = total.astype(BF16)
     hbuf[0] = mine
     last = remote(hbuf.at[0], hbuf.at[1], f_sem, 0, 0, ep, other)
@@ -286,18 +334,9 @@
     out_ref[:, :half] = jnp.where(tp == 0, mine, theirs)
     out_ref[:, half:] = jnp.where(tp == 0, theirs, mine)
 
-    swap.wait_send()
+    for sent in summed:
+        sent.wait_send()
     last.wait_send()
-    for o in range(1, nz):
-        meta_out[o].wait_send()
-        z_out[o].wait_send()
-        r_out[o].wait_send()
-    for c in range(2):
-
-        @pl.loop(1, np_)
-        def _(d):
-            d_copy(c, d, me).wait_send()
-            b_copy(c, d, me).wait_send()
 
 
 def moe(nz, ng, gated, meta, wout, tok, gain, wg, wu, wd):
@@ -307,33 +346,36 @@
     vmem = pl.BlockSpec(memory_space=pltpu.VMEM)
     hbm = pl.BlockSpec(memory_space=pltpu.HBM)
 
+    sizes = (half, half // 2, half // 2)
+
     def sems(*n):
         return pltpu.SemaphoreType.DMA(n)
 
     return pl.pallas_call(
         functools.partial(moe_kernel, nz, ng),
         out_shape=jax.ShapeDtypeStruct((count, width), BF16),
-        in_specs=[vmem] * 2 + [hbm] * 6,
+        in_specs=[hbm] * 8,
         out_specs=vmem,
-        scratch_shapes=[pltpu.VMEM(a.shape, a.dtype) for a in (wout, tok, gain, wg, wu, wd)]
+        scratch_shapes=[pltpu.VMEM(a.shape, a.dtype) for a in (gated, wout, tok, gain, wg, wu, wd)]
         + [
             pltpu.VMEM((2, count, width), BF16),
             pltpu.VMEM((nz, *meta.shape), F32),
             pltpu.VMEM((nz, rows, half), BF16),
             pltpu.VMEM((2, ng, nz, half), BF16),
             pltpu.VMEM((2, 2, ng, nz, half), BF16),
-            pltpu.VMEM((2, 2, ng, nz, half), BF16),
-            pltpu.VMEM((2, 2, ng, nz, half), BF16),
-            pltpu.VMEM((nz, rows, half), BF16),
-            pltpu.VMEM((nz, rows, half), BF16),
+        ]
+        + [pltpu.VMEM((2, ng, nz, n), BF16) for n in sizes] * 2
+        + [pltpu.VMEM((nz // 2, rows, n), BF16) for n in sizes]
+        + [pltpu.VMEM((nz, rows, n), BF16) for n in sizes]
+        + [
             pltpu.VMEM((2, count, half), BF16),
-            sems(6),
+            sems(8),
             sems(2, 1),
             sems(2, nz),
             sems(2, nz),
             sems(2, 2, 2 * ng),
-            sems(2, 2, 2 * ng),
-            sems(2, nz),
+            sems(3, 2, 2 * ng),
+            sems(3, 2, nz),
             sems(2, 1),
         ],
         compiler_params=pltpu.CompilerParams(
@@ -413,7 +455,7 @@
     ]
     reads = [pltpu.make_async_copy(mem_hbm.at[b], mem.at[b], in_sem.at[b]) for b in range(count)]
     writes = [pltpu.make_async_copy(mem.at[b], nmem_hbm.at[b], out_sem.at[b]) for b in range(count)]
-    for copy in small + loads + reads:
+    for copy in small + loads[:3]:
         copy.start()
 
     for copy in small:
@@ -459,10 +501,16 @@
         loads[i].wait()
         return jnp.dot(normed, w[...], preferred_element_type=F32)
 
+    third = count // 3
     key = project(0, wk) * dim ** (-0.5)
+    for copy in reads[:third]:
+        copy.start()
     value = project(1, wv)
+    for copy in reads[third : 2 * third]:
+        copy.start()
     query = project(2, wq)
-    outgate = project(3, wo)
+    for copy in reads[2 * third :] + loads[3:]:
+        copy.start()
     query_t = query.T
     stab = stab_ref[...].T
     new_stabs = []
@@ -490,17 +538,21 @@
     for h in range(1, heads):
         both_stabs = jnp.where(heads_at == h, new_stabs[h], both_stabs)
     nstab_ref[...] = both_stabs.T
+    block = 64
     for b in range(count):
         reads[b].wait()
         for h in range(heads):
-            new = keeps[h][b : b + 1, :] * mem[b, h] + (
-                keys_t[h][:, b : b + 1] * values[h][b : b + 1, :]
-            )
-            mem[b, h] = new
-            num[h, b : b + 1, :] = jnp.sum(
-                query_t[h * dim : (h + 1) * dim, b : b + 1] * new, axis=0, keepdims=True
-            )
+            kept = keeps[h][b : b + 1, :]
+            added = values[h][b : b + 1, :]
+            folded = jnp.zeros((8, dim), F32)
+            for d in range(0, dim, block):
+                new = kept * mem[b, h, d : d + block, :] + keys_t[h][d : d + block, b : b + 1] * added
+                mem[b, h, d : d + block, :] = new
+                read = query_t[h * dim + d : h * dim + d + block, b : b + 1] * new
+                folded = folded + jnp.sum(read.reshape(block // 8, 8, dim), axis=0)
+            num[h, b : b + 1, :] = jnp.sum(folded, axis=0, keepdims=True)
         writes[b].start()
+    outgate = project(3, wo)
     local_width = heads * dim
     parts = local_width // 128
     gains = jnp.concatenate(

time: 72.6 us -> 70 us (0.964)
  the two profiles are of different devices: /device:TPU:36 before, /device:TPU:4 now
where the time goes in v3:
time: 70 us; the launch traced here: 69.9 us
  Pallas kernels  67.8 us (97%)
  local copies, waits for them, and re-layouts  1.47 us (2%)
    pallas_call x1, Pallas kernels, moe(): pl.pallas_call(functools.partial(moe_kernel, nz, ng), out_shape=jax.Shape...  58.2 us
    pallas_call x1, Pallas kernels, cell(): pl.pallas_call(cell_kernel, out_shape=(jax.ShapeDtypeStruct((count, weigh...  9.61 us
    unnamed x1, local copies, waits for them, and re-layouts  1.47 us

profile of v3, /device:TPU:4, one launch (start us, length us, event | category | flops | bytes accessed | tf_op | source)
XLA Modules:
  0.0 69.9 jit_solution(9554069973879797159)
XLA Ops:
  0.6 9.6 %cell.1 = (bf16[12,384]{1,0:T(8,128)(2,1)}, f32[24,128]{1,0:T(8,128)}, f32[12,2,192]{2,1,0:T(2,128)}, f32[2,12]{1,0:T(2,128)}, f32[12,2,192,192]{3,2,1,0:T(8,128)}) custom-call(bf16[12,2048]{1,0:T(8,128)(2,1)} %tok_hbm.3, f32[1,2048]{1,0:T(1,128)} %bitcast.18, bf16[4,2048]{1,0:T(4,128)(2,1)} %bitcast.16, bf16[4,2048]{1,0:T(4,128)(2,1)} %bitcast.17, ...), custom_call_target="tpu_custom_call" | custom-call | tf_op jit(solution)/shard_map/cell/pallas_call | solution.py:584
  10.2 58.2 %experts.1 = bf16[12,2048]{1,0:T(8,128)(2,1)} custom-call(bf16[12,384]{1,0:T(8,128)(2,1)} %get-tuple-element.9.gated_hbm, f32[24,128]{1,0:T(8,128)} %get-tuple-element.10.meta_hbm, bf16[384,2048]{1,0:T(8,128)(2,1)} %wout_hbm.1, bf16[12,2048]{1,0:T(8,128)(2,1)} %tok_hbm.3, f32[1,2048]{1,0:T(1,128)} %bitcast.19, bf16[2048,512]{1,0:T(8,128)(2,1)} %bitcast.13, ...), custom_call_target="tpu_custom_call" | custom-call | tf_op jit(solution)/shard_map/experts/pallas_call | solution.py:354
  68.4 1.5 %copy.25 = bf16[12,2048]{1,0:T(8,128)(2,1)} copy(bf16[12,2048]{1,0:T(8,128)(2,1)} %experts.1) | data formatting | bytes 98304

commit v4 on v3

--- a/solution.py
+++ b/solution.py
@@ -9,7 +9,7 @@
 
 EPS = 1e-06
 PLANE = 16
-FULL_VMEM = 67043328
+MOST_VMEM = 67043328 - (1 << 20)
 BF16 = jnp.bfloat16
 F32 = jnp.float32
 
@@ -28,8 +28,8 @@
 def moe_kernel(
     nz,
     ng,
-    gated_hbm,
-    meta_hbm,
+    gated_ref,
+    meta_ref,
     wout_hbm,
     tok_hbm,
     gain_hbm,
@@ -37,7 +37,6 @@
     wu_hbm,
     wd_hbm,
     out_ref,
-    gated_ref,
     wout,
     tok_ref,
     gain_ref,
@@ -87,9 +86,7 @@
         pltpu.make_async_copy(src, dst, w_sem.at[i])
         for i, (src, dst) in enumerate(
             (
-                (gated_hbm, gated_ref),
                 (wout_hbm, wout),
-                (meta_hbm, meta.at[0]),
                 (tok_hbm, tok_ref),
                 (gain_hbm, gain_ref),
                 (wg_hbm, wg),
@@ -98,8 +95,8 @@
             )
         )
     ]
-    weights = copies[5:]
-    for copy in copies[:5]:
+    weights = copies[3:]
+    for copy in copies[:3]:
         copy.start()
 
     barrier = pltpu.get_barrier_semaphore()
@@ -113,12 +110,12 @@
         q = lax.rem(me + d, np_)
         pl.semaphore_signal(barrier, inc=1, device_id=(z * ng + q // 2, q % 2))
 
+    meta[0] = meta_ref[...]
     copies[0].wait()
-    copies[1].wait()
     for copy in weights:
         copy.start()
     pbuf[0] = jnp.dot(gated_ref[...], wout[...], preferred_element_type=F32).astype(BF16)
-    for copy in copies[2:5]:
+    for copy in copies[1:3]:
         copy.wait()
     pl.semaphore_wait(barrier, nz - 1 + np_ - 1)
 
@@ -353,10 +350,10 @@
 
     return pl.pallas_call(
         functools.partial(moe_kernel, nz, ng),
-        out_shape=jax.ShapeDtypeStruct((count, width), BF16),
-        in_specs=[hbm] * 8,
+        out_shape=pltpu.VMEM((count, width), BF16),
+        in_specs=[vmem] * 2 + [hbm] * 6,
         out_specs=vmem,
-        scratch_shapes=[pltpu.VMEM(a.shape, a.dtype) for a in (gated, wout, tok, gain, wg, wu, wd)]
+        scratch_shapes=[pltpu.VMEM(a.shape, a.dtype) for a in (wout, tok, gain, wg, wu, wd)]
         + [
             pltpu.VMEM((2, count, width), BF16),
             pltpu.VMEM((nz, *meta.shape), F32),
@@ -369,7 +366,7 @@
         + [pltpu.VMEM((nz, rows, n), BF16) for n in sizes]
         + [
             pltpu.VMEM((2, count, half), BF16),
-            sems(8),
+            sems(6),
             sems(2, 1),
             sems(2, nz),
             sems(2, nz),
@@ -379,7 +376,7 @@
             sems(2, 1),
         ],
         compiler_params=pltpu.CompilerParams(
-            collective_id=0, has_side_effects=True, vmem_limit_bytes=FULL_VMEM
+            collective_id=0, has_side_effects=True, vmem_limit_bytes=MOST_VMEM
         ),
         name="experts",
     )(gated, meta, wout, tok, gain, wg, wu, wd)
@@ -403,8 +400,8 @@
     mem_hbm,
     gated_ref,
     meta_ref,
-    nnorm_ref,
-    nstab_ref,
+    nnorm_hbm,
+    nstab_hbm,
     nmem_hbm,
     tok_ref,
     ngain_ref,
@@ -422,6 +419,9 @@
     wo,
     mem,
     num,
+    nnorm_ref,
+    nstab_ref,
+    o_sem,
     s_sem,
     w_sem,
     in_sem,
@@ -455,7 +455,8 @@
     ]
     reads = [pltpu.make_async_copy(mem_hbm.at[b], mem.at[b], in_sem.at[b]) for b in range(count)]
     writes = [pltpu.make_async_copy(mem.at[b], nmem_hbm.at[b], out_sem.at[b]) for b in range(count)]
-    for copy in small + loads[:3]:
+    third = count // 3
+    for copy in small + loads[:3] + reads[:third]:
         copy.start()
 
     for copy in small:
@@ -501,16 +502,13 @@
         loads[i].wait()
         return jnp.dot(normed, w[...], preferred_element_type=F32)
 
-    third = count // 3
     key = project(0, wk) * dim ** (-0.5)
-    for copy in reads[:third]:
+    for copy in reads[third : 2 * third]:
         copy.start()
     value = project(1, wv)
-    for copy in reads[third : 2 * third]:
+    for copy in reads[2 * third :] + loads[3:]:
         copy.start()
     query = project(2, wq)
-    for copy in reads[2 * third :] + loads[3:]:
-        copy.start()
     query_t = query.T
     stab = stab_ref[...].T
     new_stabs = []
@@ -531,22 +529,35 @@
         den = jnp.sum(query[:, at] * new_norm, axis=1, keepdims=True)
         floors.append(jnp.maximum(jnp.abs(den), jnp.exp(-new_stab)))
         keeps.append(jnp.broadcast_to(keep, (count, dim)))
-        values.append(value[:, at])
-        keys_t.append(written.T)
+        key_hi = written.astype(BF16).astype(F32)
+        value_hi = value[:, at].astype(BF16).astype(F32)
+        keys_t.append(
+            jnp.concatenate([key_hi, key_hi, written - key_hi], axis=0).T.astype(BF16)
+        )
+        values.append(jnp.concatenate([value_hi, value[:, at] - value_hi, value_hi], axis=0))
     heads_at = lax.broadcasted_iota(jnp.int32, (count, heads), 1)
     both_stabs = jnp.broadcast_to(new_stabs[0], (count, heads))
     for h in range(1, heads):
         both_stabs = jnp.where(heads_at == h, new_stabs[h], both_stabs)
     nstab_ref[...] = both_stabs.T
+    results = [
+        pltpu.make_async_copy(nnorm_ref, nnorm_hbm, o_sem.at[0]),
+        pltpu.make_async_copy(nstab_ref, nstab_hbm, o_sem.at[1]),
+    ]
+    for copy in results:
+        copy.start()
+    sequence = lax.rem(lax.broadcasted_iota(jnp.int32, (3 * count, dim), 0), count)
     block = 64
     for b in range(count):
         reads[b].wait()
         for h in range(heads):
             kept = keeps[h][b : b + 1, :]
-            added = values[h][b : b + 1, :]
+            added = jnp.where(sequence == b, values[h], 0.0).astype(BF16)
             folded = jnp.zeros((8, dim), F32)
             for d in range(0, dim, block):
-                new = kept * mem[b, h, d : d + block, :] + keys_t[h][d : d + block, b : b + 1] * added
+                new = kept * mem[b, h, d : d + block, :] + jnp.dot(
+                    keys_t[h][d : d + block, :], added, preferred_element_type=F32
+                )
                 mem[b, h, d : d + block, :] = new
                 read = query_t[h * dim + d : h * dim + d + block, b : b + 1] * new
                 folded = folded + jnp.sum(read.reshape(block // 8, 8, dim), axis=0)
@@ -571,7 +582,7 @@
             * gains[:, at]
         )
         gated_ref[:, at] = (scaled * jax.nn.sigmoid(outgate[:, at])).astype(BF16)
-    for copy in writes:
+    for copy in writes + results:
         copy.wait()
 
 
@@ -584,23 +595,26 @@
     return pl.pallas_call(
         cell_kernel,
         out_shape=(
-            jax.ShapeDtypeStruct((count, weights[0].shape[1]), BF16),
-            jax.ShapeDtypeStruct((rows16 + 8, 128), F32),
+            pltpu.VMEM((count, weights[0].shape[1]), BF16),
+            pltpu.VMEM((rows16 + 8, 128), F32),
             jax.ShapeDtypeStruct(norm_shape, F32),
             jax.ShapeDtypeStruct((norm_shape[1], count), F32),
             jax.ShapeDtypeStruct(memory.shape, F32),
         ),
         in_specs=[hbm] * (len(small) + len(weights) + 1),
-        out_specs=(vmem, vmem, vmem, vmem, hbm),
+        out_specs=(vmem, vmem, hbm, hbm, hbm),
         scratch_shapes=[pltpu.VMEM(a.shape, a.dtype) for a in (*small, *weights, memory)]
         + [
             pltpu.VMEM((norm_shape[1], count, norm_shape[2]), F32),
+            pltpu.VMEM(norm_shape, F32),
+            pltpu.VMEM((norm_shape[1], count), F32),
+            pltpu.SemaphoreType.DMA((2,)),
             pltpu.SemaphoreType.DMA((len(small),)),
             pltpu.SemaphoreType.DMA((len(weights),)),
             pltpu.SemaphoreType.DMA((count,)),
             pltpu.SemaphoreType.DMA((count,)),
         ],
-        compiler_params=pltpu.CompilerParams(vmem_limit_bytes=FULL_VMEM),
+        compiler_params=pltpu.CompilerParams(vmem_limit_bytes=MOST_VMEM),
         name="cell",
     )(*small, *weights, memory)
 
@@ -646,6 +660,8 @@
         (w_query, w_key, w_value, w_outgate),
         memory,
     )
+    gated = pltpu.with_memory_space_constraint(gated, pltpu.VMEM)
+    meta = pltpu.with_memory_space_constraint(meta, pltpu.VMEM)
     next_tokens = moe(
         nz,
         ng,

time: 70 us -> 67.3 us (0.961)
  Pallas kernels: 67.8 us -> 65.9 us
  local copies, waits for them, and re-layouts: 1.47 us -> 0.63 us
    pallas_call x2, Pallas kernels: 67.8 us -> 65.9 us  [the longest x1 57.8 us: moe(): pl.pallas_call(functools.partial(moe_kernel, nz, ng), out_shape=pltpu.VME...]
    unnamed x1, local copies, waits for them, and re-layouts: 1.47 us -> 0.63 us
where the time goes in v4:
time: 67.3 us; the launch traced here: 67.2 us
  Pallas kernels  65.9 us (98%)
    pallas_call x1, Pallas kernels, moe(): pl.pallas_call(functools.partial(moe_kernel, nz, ng), out_shape=pltpu.VME...  57.8 us
    pallas_call x1, Pallas kernels, cell(): pl.pallas_call(cell_kernel, out_shape=(pltpu.VMEM((count, weights[0].shap...  8.05 us

profile of v4, /device:TPU:4, one launch (start us, length us, event | category | flops | bytes accessed | tf_op | source)
XLA Modules:
  0.0 67.2 jit_solution(3524161554003852344)
XLA Ops:
  0.6 8.0 %cell.1 = (bf16[12,384]{1,0:T(8,128)(2,1)S(1)}, f32[24,128]{1,0:T(8,128)S(1)}, f32[12,2,192]{2,1,0:T(2,128)}, f32[2,12]{1,0:T(2,128)}, f32[12,2,192,192]{3,2,1,0:T(8,128)}) custom-call(bf16[12,2048]{1,0:T(8,128)(2,1)} %tok_hbm.3, f32[1,2048]{1,0:T(1,128)} %bitcast.18, bf16[4,2048]{1,0:T(4,128)(2,1)} %bitcast.16, bf16[4,2048]{1,0:T(4,128)(2,1)} %bitcast.17, ...), custom_call_target="tpu_custom_call" | custom-call | tf_op jit(solution)/shard_map/cell/pallas_call | solution.py:595
  8.7 57.8 %experts.1 = bf16[12,2048]{1,0:T(8,128)(2,1)S(1)} custom-call(bf16[12,384]{1,0:T(8,128)(2,1)S(1)} %get-tuple-element.9.gated_ref, f32[24,128]{1,0:T(8,128)S(1)} %get-tuple-element.10.meta_ref, bf16[384,2048]{1,0:T(8,128)(2,1)} %wout_hbm.1, bf16[12,2048]{1,0:T(8,128)(2,1)} %tok_hbm.3, f32[1,2048]{1,0:T(1,128)} %bitcast.19, bf16[2048,512]{1,0:T(8,128)(2,1)} %bitcast.13, ...), custom_call_target="tpu_custom_call" | custom-call | tf_op jit(solution)/shard_map/experts/pallas_call | solution.py:351
  66.5 0.6 copy.25

commit v5 on v4

--- a/solution.py
+++ b/solution.py
@@ -78,7 +78,8 @@
     other = 1 - tp
     np_ = 2 * ng
     count, width = tok_ref.shape
-    rows, half = zrows.shape[1:]
+    rows = meta.shape[1] - 8
+    half = width // 2
     per = nz // 2
     slots = 2 * per
 
@@ -152,9 +153,16 @@
     def my_half(values):
         return jnp.where(tp == 0, values[:, :half], values[:, half:])
 
-    if rows > count:
-        zrows[0] = jnp.zeros((rows, half), BF16)
-    zrows[0, :count, :] = my_half(ffn_in)
+    def stacked(values):
+        n = values.shape[1] // 4
+        quarters = [values[:, q * n : (q + 1) * n] for q in range(4)]
+        return jnp.concatenate(quarters, axis=0).astype(BF16)
+
+    def unstacked(values):
+        floats = values.astype(F32)
+        return jnp.concatenate([floats[q * count : (q + 1) * count] for q in range(4)], axis=1)
+
+    zrows[0] = stacked(my_half(ffn_in.astype(F32)))
     z_out, z_in = along_z(z_sem, lambda o: zrows.at[0], lambda o: zrows.at[o])
     for o in range(1, nz):
         z_out[o].start()
@@ -166,22 +174,19 @@
     lanes = per * rows
     picks, mixes = [], []
     for c in range(2):
-        whole = [
-            meta[c * per + i, rows:, :] if i == 0 else pltpu.roll(meta[c * per + i, rows:, :], i * rows, 1)
-            for i in range(per)
-        ]
-        by_lane = whole[0]
-        for part in whole[1:]:
-            by_lane = by_lane + part
-        source = lax.broadcasted_iota(jnp.int32, (4, lanes), 1) // rows
-        slot_t = (
-            (by_lane[0:4, :lanes] - first) * slots + by_lane[4:8, :lanes]
-        ).astype(jnp.int32) + 2 * source
-        slot_at = lax.broadcasted_iota(jnp.int32, (ng * slots, lanes), 0)
-        pick = jnp.zeros((ng * slots, lanes), F32)
+        by_lane = jnp.concatenate(
+            [meta[c * per + i, rows:, : 4 * count] for i in range(per)], axis=1
+        )
+        lane = lax.broadcasted_iota(jnp.int32, (4, 4 * count * per), 1)
+        slot_t = ((by_lane[0:4] - first) * slots + by_lane[4:8]).astype(jnp.int32) + 2 * (
+            lane // (4 * count)
+        )
+        slot_at = lax.broadcasted_iota(jnp.int32, (ng * slots, 4 * count * per), 0)
+        pick = jnp.zeros((ng * slots, 4 * count * per), F32)
         for k in range(4):
             pick = pick + jnp.where(slot_at == slot_t[k : k + 1, :], 1.0, 0.0)
-        picks.append(pick.astype(BF16))
+        quarter = lax.rem(lax.broadcasted_iota(jnp.int32, pick.shape, 1), 4 * count) // count
+        picks.append([jnp.where(quarter == q, pick, 0.0).astype(BF16) for q in range(4)])
         by_row = meta[c * per : (c + 1) * per, :rows, :].reshape(lanes, meta.shape[2])
         source = lax.broadcasted_iota(jnp.int32, (lanes, 4), 0) // rows
         slot_r = ((by_row[:, 0:4] - first) * slots + by_row[:, 8:12]).astype(jnp.int32) + 2 * source
@@ -208,12 +213,13 @@
     for c in range(2):
         for o in range(max(1, c * per), (c + 1) * per):
             z_in[o].wait_recv()
-        gathered = zrows[c * per : (c + 1) * per].reshape(lanes, half)
-        snd[c] = (
-            jnp.dot(picks[c], gathered, preferred_element_type=F32)
-            .astype(BF16)
-            .reshape(ng, slots, half)
-        )
+        gathered = zrows[c * per : (c + 1) * per].reshape(4 * count * per, half // 4)
+        for q in range(4):
+            snd[c, :, :, q * (half // 4) : (q + 1) * (half // 4)] = (
+                jnp.dot(picks[c][q], gathered, preferred_element_type=F32)
+                .astype(BF16)
+                .reshape(ng, slots, half // 4)
+            )
 
         @pl.loop(1, np_)
         def _(d):
@@ -302,7 +308,8 @@
         sums = jnp.dot(mix_hi, served, preferred_element_type=F32) + jnp.dot(
             mix_lo, served, preferred_element_type=F32
         )
-        zsnd[u][...] = sums.astype(BF16).reshape(per, rows, size)
+        for o in range(per):
+            zsnd[u][o] = stacked(sums[o * rows : o * rows + count])
         for o in r_out:
             r_out[o].start()
             summed.append(r_out[o])
@@ -312,7 +319,7 @@
         for u in range(3):
             b_copy(u, d, me).wait_send()
 
-    total = my_half(resid).astype(F32) + zsnd[0][0, :count, :].astype(F32)
+    total = my_half(resid).astype(F32) + unstacked(zsnd[0][0])
     for d in range(1, nz):
         here, chunk = place_of(d, nz), place_of(nz - d, nz) // per
         pieces = []
@@ -320,7 +327,7 @@
             if c == chunk:
                 at = zrcv[u].at[here]
                 remote(at, at, r_sem.at[u], here, here, ep, other).wait_recv()
-                pieces.append(zrcv[u][here, :count, :].astype(F32))
+                pieces.append(unstacked(zrcv[u][here]))
         total = total + (pieces[0] if len(pieces) == 1 else jnp.concatenate(pieces, axis=1))
     mine = total.astype(BF16)
     hbuf[0] = mine
@@ -338,7 +345,6 @@
 
 def moe(nz, ng, gated, meta, wout, tok, gain, wg, wu, wd):
     count, width = tok.shape
-    rows = meta.shape[0] - 8
     half = width // 2
     vmem = pl.BlockSpec(memory_space=pltpu.VMEM)
     hbm = pl.BlockSpec(memory_space=pltpu.HBM)
@@ -357,13 +363,13 @@
         + [
             pltpu.VMEM((2, count, width), BF16),
             pltpu.VMEM((nz, *meta.shape), F32),
-            pltpu.VMEM((nz, rows, half), BF16),
+            pltpu.VMEM((nz, 4 * count, half // 4), BF16),
             pltpu.VMEM((2, ng, nz, half), BF16),
             pltpu.VMEM((2, 2, ng, nz, half), BF16),
         ]
         + [pltpu.VMEM((2, ng, nz, n), BF16) for n in sizes] * 2
-        + [pltpu.VMEM((nz // 2, rows, n), BF16) for n in sizes]
-        + [pltpu.VMEM((nz, rows, n), BF16) for n in sizes]
+        + [pltpu.VMEM((nz // 2, 4 * count, n // 4), BF16) for n in sizes]
+        + [pltpu.VMEM((nz, 4 * count, n // 4), BF16) for n in sizes]
         + [
             pltpu.VMEM((2, count, half), BF16),
             sems(6),
@@ -487,7 +493,7 @@
             by_row = jnp.where(lane == at, what, by_row)
         for at, what in ((k, code), (4 + k, rank)):
             meta_ref[rows16 + at : rows16 + at + 1, :] = jnp.sum(
-                jnp.where(lane == row, what, 0.0), axis=0, keepdims=True
+                jnp.where(lax.rem(lane, count) == row, what, 0.0), axis=0, keepdims=True
             )
     meta_ref[:count, :] = by_row
 
@@ -547,7 +553,7 @@
     for copy in results:
         copy.start()
     sequence = lax.rem(lax.broadcasted_iota(jnp.int32, (3 * count, dim), 0), count)
-    block = 64
+    block = 96
     for b in range(count):
         reads[b].wait()
         for h in range(heads):

time: 67.3 us -> 65.3 us (0.970)
  Pallas kernels: 65.9 us -> 63.9 us
    pallas_call x1, Pallas kernels: 57.8 us -> 55.9 us  [moe(): pl.pallas_call(functools.partial(moe_kernel, nz, ng), out_shape=pltpu.VME...]
where the time goes in v5:
time: 65.3 us; the launch traced here: 65.2 us
  Pallas kernels  63.9 us (98%)
    pallas_call x1, Pallas kernels, moe(): pl.pallas_call(functools.partial(moe_kernel, nz, ng), out_shape=pltpu.VME...  55.9 us
    pallas_call x1, Pallas kernels, cell(): pl.pallas_call(cell_kernel, out_shape=(pltpu.VMEM((count, weights[0].shap...  8.03 us

profile of v5, /device:TPU:4, one launch (start us, length us, event | category | flops | bytes accessed | tf_op | source)
XLA Modules:
  0.0 65.2 jit_solution(4129167625427235849)
XLA Ops:
  0.6 8.0 %cell.1 = (bf16[12,384]{1,0:T(8,128)(2,1)S(1)}, f32[24,128]{1,0:T(8,128)S(1)}, f32[12,2,192]{2,1,0:T(2,128)}, f32[2,12]{1,0:T(2,128)}, f32[12,2,192,192]{3,2,1,0:T(8,128)}) custom-call(bf16[12,2048]{1,0:T(8,128)(2,1)} %tok_hbm.3, f32[1,2048]{1,0:T(1,128)} %bitcast.18, bf16[4,2048]{1,0:T(4,128)(2,1)} %bitcast.16, bf16[4,2048]{1,0:T(4,128)(2,1)} %bitcast.17, ...), custom_call_target="tpu_custom_call" | custom-call | tf_op jit(solution)/shard_map/cell/pallas_call | solution.py:601
  8.7 55.9 %experts.1 = bf16[12,2048]{1,0:T(8,128)(2,1)S(1)} custom-call(bf16[12,384]{1,0:T(8,128)(2,1)S(1)} %get-tuple-element.9.gated_ref, f32[24,128]{1,0:T(8,128)S(1)} %get-tuple-element.10.meta_ref, bf16[384,2048]{1,0:T(8,128)(2,1)} %wout_hbm.1, bf16[12,2048]{1,0:T(8,128)(2,1)} %tok_hbm.3, f32[1,2048]{1,0:T(1,128)} %bitcast.19, bf16[2048,512]{1,0:T(8,128)(2,1)} %bitcast.13, ...), custom_call_target="tpu_custom_call" | custom-call | tf_op jit(solution)/shard_map/experts/pallas_call | solution.py:357
  64.5 0.6 copy.25

commit v6 on v5

--- a/solution.py
+++ b/solution.py
@@ -310,7 +310,7 @@
         )
         for o in range(per):
             zsnd[u][o] = stacked(sums[o * rows : o * rows + count])
-        for o in r_out:
+        for o in reversed(r_out):
             r_out[o].start()
             summed.append(r_out[o])
 
@@ -320,27 +320,34 @@
             b_copy(u, d, me).wait_send()
 
     total = my_half(resid).astype(F32) + unstacked(zsnd[0][0])
-    for d in range(1, nz):
-        here, chunk = place_of(d, nz), place_of(nz - d, nz) // per
-        pieces = []
-        for u, (c, _, _) in enumerate(units):
-            if c == chunk:
+    def arrived(u):
+        added = []
+        for d in range(1, nz):
+            if units[u][0] == place_of(nz - d, nz) // per:
+                here = place_of(d, nz)
                 at = zrcv[u].at[here]
                 remote(at, at, r_sem.at[u], here, here, ep, other).wait_recv()
-                pieces.append(unstacked(zrcv[u][here]))
-        total = total + (pieces[0] if len(pieces) == 1 else jnp.concatenate(pieces, axis=1))
-    mine = total.astype(BF16)
-    hbuf[0] = mine
-    last = remote(hbuf.at[0], hbuf.at[1], f_sem, 0, 0, ep, other)
-    last.start()
-    last.wait_recv()
-    theirs = hbuf[1]
-    out_ref[:, :half] = jnp.where(tp == 0, mine, theirs)
-    out_ref[:, half:] = jnp.where(tp == 0, theirs, mine)
+                added.append(unstacked(zrcv[u][here]))
+        return sum(added[1:], added[0]) if added else 0.0
+
+    total = total + arrived(0)
+    lasts = []
+    for f in range(2):
+        _, start, size = units[1 + f]
+        hbuf[0, f] = (total[:, start : start + size] + arrived(1 + f)).astype(BF16)
+        lasts.append(remote(hbuf.at[0, f], hbuf.at[1, f], f_sem, f, f, ep, other))
+        lasts[f].start()
+    for f in range(2):
+        _, start, size = units[1 + f]
+        lasts[f].wait_recv()
+        mine, theirs = hbuf[0, f], hbuf[1, f]
+        out_ref[:, start : start + size] = jnp.where(tp == 0, mine, theirs)
+        out_ref[:, half + start : half + start + size] = jnp.where(tp == 0, theirs, mine)
 
     for sent in summed:
         sent.wait_send()
-    last.wait_send()
+    for last in lasts:
+        last.wait_send()
 
 
 def moe(nz, ng, gated, meta, wout, tok, gain, wg, wu, wd):
@@ -371,7 +378,7 @@
         + [pltpu.VMEM((nz // 2, 4 * count, n // 4), BF16) for n in sizes]
         + [pltpu.VMEM((nz, 4 * count, n // 4), BF16) for n in sizes]
         + [
-            pltpu.VMEM((2, count, half), BF16),
+            pltpu.VMEM((2, 2, count, half // 2), BF16),
             sems(6),
             sems(2, 1),
             sems(2, nz),
@@ -379,7 +386,7 @@
             sems(2, 2, 2 * ng),
             sems(3, 2, 2 * ng),
             sems(3, 2, nz),
-            sems(2, 1),
+            sems(2, 2),
         ],
         compiler_params=pltpu.CompilerParams(
             collective_id=0, has_side_effects=True, vmem_limit_bytes=MOST_VMEM

time: 65.3 us -> 64.5 us (0.988)
  Pallas kernels: 63.9 us -> 63 us
    pallas_call x1, Pallas kernels: 55.9 us -> 54.9 us  [moe(): pl.pallas_call(functools.partial(moe_kernel, nz, ng), out_shape=pltpu.VME...]
where the time goes in v6:
time: 64.5 us; the launch traced here: 64.2 us
  Pallas kernels  63 us (98%)
  between operations  0.65 us (1%)
    pallas_call x1, Pallas kernels, moe(): pl.pallas_call(functools.partial(moe_kernel, nz, ng), out_shape=pltpu.VME...  54.9 us
    pallas_call x1, Pallas kernels, cell(): pl.pallas_call(cell_kernel, out_shape=(pltpu.VMEM((count, weights[0].shap...  8.03 us

profile of v6, /device:TPU:4, one launch (start us, length us, event | category | flops | bytes accessed | tf_op | source)
XLA Modules:
  0.0 64.2 jit_solution(4584716593551253379)
XLA Ops:
  0.6 8.0 %cell.1 = (bf16[12,384]{1,0:T(8,128)(2,1)S(1)}, f32[24,128]{1,0:T(8,128)S(1)}, f32[12,2,192]{2,1,0:T(2,128)}, f32[2,12]{1,0:T(2,128)}, f32[12,2,192,192]{3,2,1,0:T(8,128)}) custom-call(bf16[12,2048]{1,0:T(8,128)(2,1)} %tok_hbm.3, f32[1,2048]{1,0:T(1,128)} %bitcast.18, bf16[4,2048]{1,0:T(4,128)(2,1)} %bitcast.16, bf16[4,2048]{1,0:T(4,128)(2,1)} %bitcast.17, ...), custom_call_target="tpu_custom_call" | custom-call | tf_op jit(solution)/shard_map/cell/pallas_call | solution.py:608
  8.7 54.9 %experts.1 = bf16[12,2048]{1,0:T(8,128)(2,1)S(1)} custom-call(bf16[12,384]{1,0:T(8,128)(2,1)S(1)} %get-tuple-element.9.gated_ref, f32[24,128]{1,0:T(8,128)S(1)} %get-tuple-element.10.meta_ref, bf16[384,2048]{1,0:T(8,128)(2,1)} %wout_hbm.1, bf16[12,2048]{1,0:T(8,128)(2,1)} %tok_hbm.3, f32[1,2048]{1,0:T(1,128)} %bitcast.19, bf16[2048,512]{1,0:T(8,128)(2,1)} %bitcast.13, ...), custom_call_target="tpu_custom_call" | custom-call | tf_op jit(solution)/shard_map/experts/pallas_call | solution.py:364
  63.6 0.6 copy.25
